TPU v7x, 32 devices: a whole 2x2x4 slice. The times are simulated.
32 devices in a mesh: sp: 4 (over z), dp: 8 (over y, x, core).
Axes of the slice: x: 2, y: 2, z: 4, core: 2. Of those that a mesh axis runs over, the one named last changes fastest.
Arguments:
- normed: bfloat16 [8, 512, 2048], P('dp', 'sp'), may hold values from -6 to 6
- values: bfloat16 [8, 512, 2048], P('dp', 'sp'), may hold values from -6 to 6
- gate_in: bfloat16 [8, 512, 2048], P('dp', 'sp'), may hold values from -6 to 6
- step_raw: bfloat16 [8, 512, 32], P('dp', 'sp'), may hold values from -3.5 to 2.5
- upstream: bfloat16 [8, 512, 2048], P('dp', 'sp'), may hold values from -6 to 6
- proj_pair: bfloat16 [2048, 512], P('dp'), may hold values from -0.03125 to 0.03125
- conv_value: float32 [4, 2048], replicated, may hold values from -3 to 3
- conv_pair: float32 [4, 512], replicated, may hold values from -3 to 3
- step_bias: float32 [32], replicated, may hold values from -1 to 1
- decay_log: float32 [32], replicated, may hold values from -12 to -2
- skip: float32 [32], replicated, may hold values from 0.5 to 1.5
Outputs:
- grad_normed: bfloat16 [8, 512, 2048], P('dp', 'sp')
- grad_values: bfloat16 [8, 512, 2048], P('dp', 'sp')
- grad_gate: bfloat16 [8, 512, 2048], P('dp', 'sp')
- grad_step: bfloat16 [8, 512, 32], P('dp', 'sp')
- grad_proj: float32 [2048, 512], P('dp')
All inputs are finite; a program needn't handle non-finite values.
Results may differ from a plain program's by a relative error of at most 0.02.
Values may be sent and summed in bfloat16 or wider, within the bound.
A program may use at most 128 MiB of HBM per device.

v0:
```python
import functools

import jax
import jax.numpy as jnp
from jax import lax
from jax.experimental import pallas as pl
from jax.experimental.pallas import tpu as pltpu
from jax.sharding import PartitionSpec as P

HEAD = 64
STATE = 128
LANES = 128
PAIR = 2 * STATE
exact = lax.Precision.HIGHEST
f32 = jnp.float32
bf16 = jnp.bfloat16

NN = (((1,), (0,)), ((), ()))
NT = (((1,), (1,)), ((), ()))
TN = (((0,), (0,)), ((), ()))


def mm(a, b, dims):
    return lax.dot_general(a, b, dims, preferred_element_type=f32)


def mm_exact(a, b, dims):
    return lax.dot_general(a, b, dims, precision=exact, preferred_element_type=f32)


def mixer_kernel(
    sp,
    heads,
    groups,
    normed,
    values,
    gate,
    up,
    step,
    proj,
    tap_v,
    tap_p,
    bias,
    log_rate,
    skip,
    gn,
    gv,
    gg,
    gs,
    gp,
    cot,
    pair,
    rv,
    rc,
    rs,
    rp,
    xv,
    xp,
    us,
    slope_v,
    slope_p,
    bc,
    xs,
    dxl,
    dbc,
    r1s,
    acs,
    dts,
    sgs,
    st_all,
    st,
    dst_,
    dv,
    dp_,
    ybuf,
    gvbuf,
    gpbuf,
    dtbuf,
    yrec,
    prec,
    drec,
    send_sem,
    recv_sem,
):
    me = lax.axis_index("sp")
    T = values.shape[0]
    inner = values.shape[1]
    W = inner // sp
    hd = heads // sp
    tiles = W // LANES

    barrier = pltpu.get_barrier_semaphore()
    for off in range(1, sp):
        peer = lax.rem(me + off, sp)
        pl.semaphore_signal(
            barrier, inc=1, device_id={"sp": peer}, device_id_type=pl.DeviceIdType.MESH
        )
    pl.semaphore_wait(barrier, sp - 1)

    def rows(i):
        return pl.ds(pl.multiple_of(i * T, T), T)

    def cols(i):
        return pl.ds(pl.multiple_of(i * W, LANES), W)

    def group_cols(i):
        g = (i * hd) // (heads // groups)
        return pl.ds(pl.multiple_of(g * PAIR, LANES), PAIR)

    def remote(kind, src, dst, to, frm):
        return pltpu.make_async_remote_copy(
            src_ref=src,
            dst_ref=dst,
            send_sem=send_sem.at[kind, to],
            recv_sem=recv_sem.at[kind, frm],
            device_id={"sp": to},
            device_id_type=pl.DeviceIdType.MESH,
        )

    def go_values(to, frm):
        return remote(0, values.at[:, cols(to)], rv.at[rows(frm), :], to, frm)

    def go_cot(to, frm):
        return remote(1, cot.at[:, cols(to)], rc.at[rows(frm), :], to, frm)

    def go_step(to, frm):
        return remote(2, step, rs.at[rows(frm), :], to, frm)

    def go_pair(to, frm):
        return remote(3, pair.at[:, group_cols(to)], rp.at[rows(frm), :], to, frm)

    def go_y(to, frm):
        return remote(4, ybuf.at[rows(to), :], yrec.at[:, cols(frm)], to, frm)

    def go_gv(to, frm):
        return remote(5, gvbuf.at[rows(to), :], gv.at[:, cols(frm)], to, frm)

    def go_gp(to, frm):
        return remote(6, gpbuf.at[rows(to), :], prec.at[rows(frm), :], to, frm)

    def go_dt(to, frm):
        return remote(7, dtbuf.at[rows(to), :], drec.at[rows(frm), :], to, frm)

    def send_all(go):
        for off in range(1, sp):
            go(lax.rem(me + off, sp), me).start()

    send_all(go_values)
    send_all(go_step)
    rv[rows(me), :] = values[:, cols(me)]
    rs[rows(me), :] = step[...]

    @pl.loop(0, inner // 256)
    def _(j):
        at = pl.ds(pl.multiple_of(j * 256, 256), 256)
        v = gate[:, at].astype(f32)
        cot[:, at] = (up[:, at].astype(f32) * (v * jax.nn.sigmoid(v))).astype(bf16)

    send_all(go_cot)
    rc[rows(me), :] = cot[:, cols(me)]
    for g in range(groups):
        at = slice(g * PAIR, (g + 1) * PAIR)
        pair[:, at] = mm(normed[...], proj[:, at], NN).astype(bf16)
    send_all(go_pair)
    rp[rows(me), :] = pair[:, group_cols(me)]

    row_i = lax.broadcasted_iota(jnp.int32, (T, T), 0)
    col_i = lax.broadcasted_iota(jnp.int32, (T, T), 1)
    causal = row_i >= col_i
    tri = causal.astype(f32)
    lane = lax.broadcasted_iota(jnp.int32, (T, LANES), 1)
    low = lane < HEAD
    sel_r = lax.broadcasted_iota(jnp.int32, (LANES, W), 0)
    sel_c = lax.broadcasted_iota(jnp.int32, (LANES, W), 1)
    sel = (sel_c // HEAD == sel_r).astype(f32)

    def head_sum(z):
        return mm_exact(z, sel, NT)

    def spread(x, j):
        a = x[:, 2 * j : 2 * j + 1]
        b = x[:, 2 * j + 1 : 2 * j + 2]
        mask = low if x.shape[0] == T else low[0 : x.shape[0]]
        return jnp.where(mask, a, b)

    rate = -jnp.exp(log_rate[...])
    st[...] = jnp.zeros_like(st)
    dst_[...] = jnp.zeros_like(dst_)
    xv[0:8, :] = jnp.zeros((8, W), f32)
    xp[0:8, :] = jnp.zeros((8, PAIR), f32)
    dv[...] = jnp.zeros_like(dv)
    dp_[...] = jnp.zeros_like(dp_)

    def conv(buf, taps, c, at):
        win = buf[pl.ds(pl.multiple_of(c * T, 8), T + 8), at]
        total = taps[0:1, at] * win[5 : 5 + T]
        for k in range(1, 4):
            total = total + taps[k : k + 1, at] * win[5 + k : 5 + k + T]
        return total

    def conv_back(carry, grad, taps, at):
        win = jnp.concatenate([grad, carry[:, at]], axis=0)
        carry[:, at] = grad[0:8]
        total = taps[3:4, at] * win[0:T]
        for k in range(3):
            total = total + taps[k : k + 1, at] * win[3 - k : 3 - k + T]
        return total

    def silu_parts(s):
        sig = jax.nn.sigmoid(s)
        return s * sig, sig * (1.0 + s * (1.0 - sig))

    @pl.loop(0, sp)
    def _(c):
        here = rows(c)
        after8 = pl.ds(pl.multiple_of(c * T + 8, 8), T)

        @pl.when(c != me)
        def _():
            go_values(c, c).wait_recv()
            go_step(c, c).wait_recv()
            go_cot(c, c).wait_recv()
            go_pair(c, c).wait_recv()

        raw = pltpu.roll(rs[here, :].astype(f32), lax.rem(LANES - me * hd, LANES), 1) + bias[...]
        dt = jax.nn.softplus(raw)
        sgs[here, :] = jax.nn.sigmoid(raw)
        dts[here, :] = dt
        ac = mm_exact(tri, dt * rate, NN)
        acs[here, :] = ac
        ac_t = ac.T
        ea = jnp.exp(ac)
        end = ac[T - 1 : T, :]
        te = jnp.exp(end - ac)
        e_end = jnp.exp(end)

        xp[after8, :] = rp[here, :].astype(f32)
        for j in range(2):
            at = slice(j * LANES, (j + 1) * LANES)
            act, slope = silu_parts(conv(xp, tap_p, c, at))
            bc[here, at] = act.astype(bf16)
            slope_p[here, at] = slope
        b = bc[here, 0:STATE]
        cc = bc[here, STATE:PAIR]
        g = mm(cc, b, NT)
        d_g = jnp.zeros((T, T), f32)
        d_c = jnp.zeros((T, STATE), f32)
        zs = []
        for j in range(tiles):
            at = slice(j * LANES, (j + 1) * LANES)
            xv[after8, at] = rv[here, at].astype(f32)
            u, slope = silu_parts(conv(xv, tap_v, c, at))
            us[here, at] = u
            slope_v[here, at] = slope
            dy = rc[here, at]
            x = (u * spread(dt, j)).astype(bf16)
            xs[here, at] = x
            zero = jnp.zeros_like(x)
            decays = []
            mixes = []
            for q in range(2):
                h = 2 * j + q
                diff = ac[:, h : h + 1] - ac_t[h : h + 1, :]
                decay = jnp.exp(jnp.where(causal, diff, -1e30))
                decays.append(decay)
                mixes.append((g * decay).astype(bf16))
            x2 = jnp.concatenate([jnp.where(low, x, zero), jnp.where(low, zero, x)], axis=0)
            dy2 = jnp.concatenate([jnp.where(low, dy, zero), jnp.where(low, zero, dy)], axis=0)
            y = mm(jnp.concatenate(mixes, axis=1), x2, NN)
            dxl[here, at] = mm(jnp.concatenate(mixes, axis=0), dy2, TN)
            d_mix = mm(dy2, x, NT)
            d_g = d_g + d_mix[0:T] * decays[0] + d_mix[T : 2 * T] * decays[1]
            s_in = st[:, at].astype(bf16)
            st_all[pl.ds(pl.multiple_of(c * STATE, STATE), STATE), at] = s_in
            dyf = dy.astype(f32)
            eaj = spread(ea, j)
            y = y + eaj * mm(cc, s_in, NN)
            d_c = d_c + mm((eaj * dyf).astype(bf16), s_in, NT)
            zs.append(dyf * y)
            ybuf[here, at] = (y + spread(skip[...], j) * u).astype(bf16)
            xe = (x.astype(f32) * spread(te, j)).astype(bf16)
            st[:, at] = spread(e_end, j) * st[:, at] + mm(b, xe, TN)
        r1s[here, :] = head_sum(jnp.concatenate(zs, axis=1) if tiles > 1 else zs[0])
        dg = d_g.astype(bf16)
        dbc[here, 0:STATE] = mm(dg, cc, TN)
        dbc[here, STATE:PAIR] = mm(dg, b, NN) + d_c

        @pl.when(c != me)
        def _():
            go_y(c, me).start()

        @pl.when(c == me)
        def _():
            yrec[:, cols(me)] = ybuf[rows(me), :]

    @pl.loop(0, sp)
    def _(i):
        c = sp - 1 - i
        here = rows(c)
        ac = acs[here, :]
        dt = dts[here, :]
        end = ac[T - 1 : T, :]
        ea = jnp.exp(ac)
        te = jnp.exp(end - ac)
        e_end = jnp.exp(end)
        b = bc[here, 0:STATE]
        cc = bc[here, STATE:PAIR]
        d_b = dbc[here, 0:STATE]
        zs = []
        ends = []
        for j in range(tiles):
            at = slice(j * LANES, (j + 1) * LANES)
            ds = dst_[:, at]
            dsb = ds.astype(bf16)
            x = xs[here, at].astype(f32)
            tej = spread(te, j)
            xe = x * tej
            far = mm(b, dsb, NN)
            d_b = d_b + mm(xe.astype(bf16), dsb, NT)
            dx = dxl[here, at] + tej * far
            zs.append(x * dx)
            s_in = st_all[pl.ds(pl.multiple_of(c * STATE, STATE), STATE), at].astype(f32)
            ee = spread(e_end, j)
            ends.append(
                jnp.sum(xe * far, axis=0, keepdims=True)
                + ee * jnp.sum(ds * s_in, axis=0, keepdims=True)
            )
            dyf = rc[here, at].astype(f32)
            du = spread(dt, j) * dx + spread(skip[...], j) * dyf
            gvbuf[here, at] = conv_back(dv, du * slope_v[here, at], tap_v, at).astype(bf16)
            dst_[:, at] = ee * ds + mm(cc, (spread(ea, j) * dyf).astype(bf16), TN)
        z = jnp.concatenate(zs, axis=1) if tiles > 1 else zs[0]
        z_end = jnp.concatenate(ends, axis=1) if tiles > 1 else ends[0]
        xd = head_sum(z)
        d_end = head_sum(jnp.broadcast_to(z_end, (8, W)))[0:1, :]
        d_ac = r1s[here, :] - xd
        back = mm_exact(tri, d_ac, TN) + d_end
        d_dt = (xd / dt + rate * back) * sgs[here, :]
        d_dt = jnp.where(lane < hd, d_dt, 0.0)
        dtbuf[here, :] = pltpu.roll(d_dt, me * hd, 1).astype(bf16)
        for j, part in enumerate((d_b, dbc[here, STATE:PAIR])):
            at = slice(j * LANES, (j + 1) * LANES)
            gpbuf[here, at] = conv_back(dp_, part * slope_p[here, at], tap_p, at).astype(bf16)

        @pl.when(c != me)
        def _():
            go_gp(c, me).start()
            go_gv(c, me).start()
            go_dt(c, me).start()

        @pl.when(c == me)
        def _():
            gv[:, cols(me)] = gvbuf[rows(me), :]
            prec[rows(me), :] = gpbuf[rows(me), :]
            drec[rows(me), :] = dtbuf[rows(me), :]

    def wait_all(go):
        for off in range(1, sp):
            frm = lax.rem(me + off, sp)
            go(frm, frm).wait_recv()

    wait_all(go_y)

    @pl.loop(0, inner // 256)
    def _(j):
        at = pl.ds(pl.multiple_of(j * 256, 256), 256)
        v = gate[:, at].astype(f32)
        sig = jax.nn.sigmoid(v)
        gg[:, at] = (
            up[:, at].astype(f32) * yrec[:, at].astype(f32) * (sig * (1.0 + v * (1.0 - sig)))
        ).astype(bf16)

    wait_all(go_gp)
    totals = []
    for g in range(groups):
        total = None
        for k in range(sp):
            if (k * hd) // (heads // groups) == g:
                term = prec[k * T : (k + 1) * T, :].astype(f32)
                total = term if total is None else total + term
        totals.append(total.astype(bf16))
    dpair = jnp.concatenate(totals, axis=1)
    for j in range(normed.shape[1] // 512):
        at = slice(j * 512, (j + 1) * 512)
        gp[at, :] = mm(normed[:, at], dpair, TN).astype(bf16)
    for j in range(normed.shape[1] // 512):
        at = slice(j * 512, (j + 1) * 512)
        gn[:, at] = mm(dpair, proj[at, :], NT).astype(bf16)
    wait_all(go_dt)
    total = drec[0:T, :].astype(f32)
    for k in range(1, sp):
        total = total + drec[k * T : (k + 1) * T, :].astype(f32)
    gs[...] = total.astype(bf16)
    wait_all(go_gv)
    for go in (go_values, go_cot, go_step, go_pair, go_y, go_gv, go_gp, go_dt):
        for off in range(1, sp):
            to = lax.rem(me + off, sp)
            go(to, me).wait_send()


def per_device(
    normed,
    values,
    gate_in,
    step_raw,
    upstream,
    proj_pair,
    conv_value,
    conv_pair,
    step_bias,
    decay_log,
    skip,
):
    sp = lax.axis_size("sp")
    me = lax.axis_index("sp")
    T = normed.shape[1]
    width = normed.shape[2]
    inner = values.shape[2]
    heads = step_raw.shape[2]
    groups = proj_pair.shape[1] // PAIR
    hd = heads // sp
    W = inner // sp
    L = T * sp
    dp = lax.axis_size("dp")

    def share(block, axis, count):
        copies = jnp.broadcast_to(block[None], (count,) + block.shape)
        return lax.all_to_all(copies, axis, split_axis=0, concat_axis=0, tiled=True)

    full_proj = share(proj_pair, "dp", dp).reshape(-1, proj_pair.shape[1])
    group = (me * hd) // (heads // groups)
    tap_v = lax.dynamic_slice_in_dim(conv_value, me * W, W, 1)
    tap_p = lax.dynamic_slice_in_dim(conv_pair, group * PAIR, PAIR, 1)

    def local(vec):
        part = lax.dynamic_slice_in_dim(vec, me * hd, hd, 0)
        return jnp.pad(part, (0, LANES - hd))[None]

    step = jnp.pad(step_raw[0], ((0, 0), (0, LANES - heads)))
    vmem = pl.BlockSpec(memory_space=pltpu.VMEM)
    V = pltpu.VMEM
    scratch = [
        V((T, inner), bf16),
        V((T, groups * PAIR), bf16),
        V((L, W), bf16),
        V((L, W), bf16),
        V((L, LANES), bf16),
        V((L, PAIR), bf16),
        V((L + 8, W), f32),
        V((L + 8, PAIR), f32),
        V((L, W), f32),
        V((L, W), f32),
        V((L, PAIR), f32),
        V((L, PAIR), bf16),
        V((L, W), bf16),
        V((L, W), f32),
        V((L, PAIR), f32),
        V((L, LANES), f32),
        V((L, LANES), f32),
        V((L, LANES), f32),
        V((L, LANES), f32),
        V((sp * STATE, W), bf16),
        V((STATE, W), f32),
        V((STATE, W), f32),
        V((8, W), f32),
        V((8, PAIR), f32),
        V((L, W), bf16),
        V((L, W), bf16),
        V((L, PAIR), bf16),
        V((L, LANES), bf16),
        V((T, inner), bf16),
        V((L, PAIR), bf16),
        V((L, LANES), bf16),
        pltpu.SemaphoreType.DMA((8, sp)),
        pltpu.SemaphoreType.DMA((8, sp)),
    ]
    gn, gv, gg, gs, gp = pl.pallas_call(
        functools.partial(mixer_kernel, sp, heads, groups),
        out_shape=(
            jax.ShapeDtypeStruct((T, width), bf16),
            jax.ShapeDtypeStruct((T, inner), bf16),
            jax.ShapeDtypeStruct((T, inner), bf16),
            jax.ShapeDtypeStruct((T, LANES), bf16),
            jax.ShapeDtypeStruct((width, groups * PAIR), bf16),
        ),
        in_specs=[vmem] * 11,
        out_specs=(vmem,) * 5,
        scratch_shapes=scratch,
        compiler_params=pltpu.CompilerParams(
            collective_id=0, has_side_effects=True, vmem_limit_bytes=50 * 1024 * 1024
        ),
    )(
        normed[0],
        values[0],
        gate_in[0],
        upstream[0],
        step,
        full_proj,
        tap_v,
        tap_p,
        local(step_bias),
        local(decay_log),
        local(skip),
    )
    terms = lax.all_to_all(
        gp.reshape((dp,) + proj_pair.shape), "dp", split_axis=0, concat_axis=0, tiled=True
    )
    grad_rows = terms.astype(f32).sum(axis=0).astype(bf16)
    grad_proj = share(grad_rows, "sp", sp).astype(f32).sum(axis=0)
    return (gn[None], gv[None], gg[None], gs[None, :, :heads], grad_proj)


def solution(mesh):
    tok = P("dp", "sp", None)
    in_specs = (tok, tok, tok, tok, tok, P("dp", None), P(), P(), P(), P(), P())
    out_specs = (tok, tok, tok, tok, P("dp", None))
    return jax.shard_map(
        per_device, mesh=mesh, in_specs=in_specs, out_specs=out_specs, check_vma=False
    )
```

profile of v0, /device:TPU:0, one launch (start us, length us, event | category | flops | bytes accessed | tf_op | source)
XLA Modules:
  0.0 172.1 jit_solution(14693741715747180642)
XLA Ops:
  0.6 0.0 copy-start
  0.6 2.4 %broadcast_in_dim.33 = bf16[8,256,512]{2,1,0:T(8,128)(2,1)} broadcast(bf16[256,512]{1,0:T(8,128)(2,1)} %param.16), dimensions={1,2} | broadcast | bytes 2359296 | tf_op jit(solution)/shard_map/broadcast_in_dim | solution.py:427
  3.1 0.0 copy-start.9
  3.1 0.0 copy-start.10
  3.1 0.0 copy-start.11
  3.1 0.0 copy-start.7
  3.1 0.0 copy-start.8
  3.1 0.0 copy-start.1
  3.1 0.0 copy-start.2
  3.1 0.0 copy-start.3
  3.2 0.0 copy-start.4
  3.2 5.3 %all-to-all-start = ((bf16[8,256,512]{2,1,0:T(8,128)(2,1)}), bf16[8,256,512]{2,1,0:T(8,128)(2,1)}, u32[]{:S(2)}, u32[]{:S(2)}) async-start(bf16[8,256,512]{2,1,0:T(8,128)(2,1)} %broadcast_in_dim.33), calls=%async_computation | async-start | bytes 4194304 | tf_op jit(solution)/shard_map/all_to_all | solution.py:428
  8.5 0.0 copy-done.9
  8.5 0.1 dynamic_slice.17
  8.6 0.0 copy-done.10
  8.6 0.1 dynamic_slice.18
  8.7 0.0 copy-done.11
  8.7 0.1 dynamic_slice.19
  8.7 0.0 copy-done.7
  8.8 0.1 copy.18
  8.9 0.0 copy-done.8
  8.9 0.0 copy-done
  9.0 26.3 %all-to-all-done = bf16[8,256,512]{2,1,0:T(8,128)(2,1)} async-done(((bf16[8,256,512]{2,1,0:T(8,128)(2,1)}), bf16[8,256,512]{2,1,0:T(8,128)(2,1)}, u32[]{:S(2)}, u32[]{:S(2)}) %all-to-all-start) | async-done | bytes 2097184 | tf_op jit(solution)/shard_map/all_to_all | solution.py:428
  35.2 0.0 copy-done.1
  35.2 0.0 copy-done.2
  35.2 0.0 copy-done.3
  35.2 0.0 copy-done.4
  35.2 67.5 %shard_map.146 = (bf16[128,2048]{1,0:T(8,128)(2,1)S(1)}, bf16[128,2048]{1,0:T(8,128)(2,1)S(1)}, bf16[128,2048]{1,0:T(8,128)(2,1)S(1)}, bf16[128,128]{1,0:T(8,128)(2,1)S(1)}, bf16[2048,512]{1,0:T(8,128)(2,1)}) custom-call(bf16[128,2048]{1,0:T(8,128)(2,1)S(1)} %bitcast.18, bf16[128,2048]{1,0:T(8,128)(2,1)S(1)} %bitcast.19, bf16[128,2048]{1,0:T(8,128)(2,1)S(1)} %bitcast.20, ...), custom_call_target="tpu_custom_call" | custom-call | tf_op jit(solution)/shard_map/pallas_call | solution.py:477
  102.7 0.0 copy-start.5
  102.7 0.8 copy-done.5
  103.5 31.5 %all_to_all.15 = bf16[8,256,512]{2,1,0:T(8,128)(2,1)S(1)} all-to-all(bf16[8,256,512]{2,1,0:T(8,128)(2,1)} %bitcast.25), channel_id=1, replica_groups=mesh['sp'=4,'dp'=8] {'dp'}, dimensions={0} | all-to-all | bytes 4194304 | tf_op jit(solution)/shard_map/all_to_all | solution.py:505
  135.0 0.4 reduce_sum.21
  135.4 1.1 broadcast_in_dim.41
  136.5 0.0 copy-start.6
  136.5 7.1 %all-to-all-start.2 = ((bf16[4,256,512]{2,1,0:T(8,128)(2,1)}), bf16[4,256,512]{2,1,0:T(8,128)(2,1)S(1)}, u32[]{:S(2)}, u32[]{:S(2)}) async-start(bf16[4,256,512]{2,1,0:T(8,128)(2,1)} %broadcast_in_dim.41), calls=%async_computation.2 | async-start | bytes 2097152 | tf_op jit(solution)/shard_map/all_to_all | solution.py:428
  143.6 0.7 copy.19
  144.3 24.5 %all-to-all-done.2 = bf16[4,256,512]{2,1,0:T(8,128)(2,1)S(1)} async-done(((bf16[4,256,512]{2,1,0:T(8,128)(2,1)}), bf16[4,256,512]{2,1,0:T(8,128)(2,1)S(1)}, u32[]{:S(2)}, u32[]{:S(2)}) %all-to-all-start.2) | async-done | bytes 1048608 | tf_op jit(solution)/shard_map/all_to_all | solution.py:428
  168.8 0.9 convert_reduce_fusion
  169.7 0.0 copy-done.6
  169.7 0.8 copy.23
  170.5 0.8 copy.24
  171.3 0.8 copy.25
  (6 shorter events, 0.0 us)
Async XLA Ops:
  0.6 8.3 %copy-start = (f32[4,2048]{1,0:T(4,128)S(1)}, f32[4,2048]{1,0:T(4,128)}, u32[]{:S(2)}) copy-start(f32[4,2048]{1,0:T(4,128)} %param.17) | copy-start | bytes 98308
  3.1 5.4 %copy-start.9 = (f32[32]{0:T(128)S(1)}, f32[32]{0:T(128)}, u32[]{:S(2)}) copy-start(f32[32]{0:T(128)} %param.19) | copy-start | bytes 388
  3.1 5.5 %copy-start.10 = (f32[32]{0:T(128)S(1)}, f32[32]{0:T(128)}, u32[]{:S(2)}) copy-start(f32[32]{0:T(128)} %param.20) | copy-start | bytes 388
  3.1 5.6 %copy-start.11 = (f32[32]{0:T(128)S(1)}, f32[32]{0:T(128)}, u32[]{:S(2)}) copy-start(f32[32]{0:T(128)} %param.21) | copy-start | bytes 388
  3.1 5.6 %copy-start.7 = (bf16[1,128,32]{1,2,0:T(8,128)(2,1)S(1)}, bf16[1,128,32]{1,2,0:T(8,128)(2,1)}, u32[]{:S(2)}) copy-start(bf16[1,128,32]{1,2,0:T(8,128)(2,1)} %param.14) | copy-start | bytes 24580
  3.1 5.8 %copy-start.8 = (f32[4,512]{1,0:T(4,128)S(1)}, f32[4,512]{1,0:T(4,128)}, u32[]{:S(2)}) copy-start(f32[4,512]{1,0:T(4,128)} %param.18) | copy-start | bytes 24580
  3.1 32.1 %copy-start.1 = (bf16[1,128,2048]{2,1,0:T(8,128)(2,1)S(1)}, bf16[1,128,2048]{2,1,0:T(8,128)(2,1)}, u32[]{:S(2)}) copy-start(bf16[1,128,2048]{2,1,0:T(8,128)(2,1)} %param.11) | copy-start | bytes 1572868
  3.1 32.1 %copy-start.2 = (bf16[1,128,2048]{2,1,0:T(8,128)(2,1)S(1)}, bf16[1,128,2048]{2,1,0:T(8,128)(2,1)}, u32[]{:S(2)}) copy-start(bf16[1,128,2048]{2,1,0:T(8,128)(2,1)} %param.12) | copy-start | bytes 1572868
  3.1 32.1 %copy-start.3 = (bf16[1,128,2048]{2,1,0:T(8,128)(2,1)S(1)}, bf16[1,128,2048]{2,1,0:T(8,128)(2,1)}, u32[]{:S(2)}) copy-start(bf16[1,128,2048]{2,1,0:T(8,128)(2,1)} %param.13) | copy-start | bytes 1572868
  3.2 32.1 %copy-start.4 = (bf16[1,128,2048]{2,1,0:T(8,128)(2,1)S(1)}, bf16[1,128,2048]{2,1,0:T(8,128)(2,1)}, u32[]{:S(2)}) copy-start(bf16[1,128,2048]{2,1,0:T(8,128)(2,1)} %param.15) | copy-start | bytes 1572868
  3.2 32.1 %all-to-all-start = ((bf16[8,256,512]{2,1,0:T(8,128)(2,1)}), bf16[8,256,512]{2,1,0:T(8,128)(2,1)}, u32[]{:S(2)}, u32[]{:S(2)}) async-start(bf16[8,256,512]{2,1,0:T(8,128)(2,1)} %broadcast_in_dim.33), calls=%async_computation | async-start | bytes 4194304 | tf_op jit(solution)/shard_map/all_to_all | solution.py:428
  102.7 0.8 copy-start.5
  136.5 33.2 %copy-start.6 = (bf16[128,2048]{1,0:T(8,128)(2,1)S(1)}, bf16[128,2048]{1,0:T(8,128)(2,1)}, u32[]{:S(2)}) copy-start(bf16[128,2048]{1,0:T(8,128)(2,1)} %copy-done.5) | copy-start | bytes 1572868
  136.5 32.3 %all-to-all-start.2 = ((bf16[4,256,512]{2,1,0:T(8,128)(2,1)}), bf16[4,256,512]{2,1,0:T(8,128)(2,1)S(1)}, u32[]{:S(2)}, u32[]{:S(2)}) async-start(bf16[4,256,512]{2,1,0:T(8,128)(2,1)} %broadcast_in_dim.41), calls=%async_computation.2 | async-start | bytes 2097152 | tf_op jit(solution)/shard_map/all_to_all | solution.py:428
where the time goes:
time: 172 us
  Pallas kernels  67.5 us (39%)
  waiting for transfers between devices  50.7 us (29%)
  blocking collectives  31.5 us (18%)
  starting transfers between devices  12.4 us (7%)
  local copies, waits for them, and re-layouts  7.8 us (5%)
    pallas_call x1, Pallas kernels, per_device(): pl.pallas_call(functools.partial(mixer_kernel, sp, heads, groups), out_sh...  67.5 us
    all_to_all x2, waiting for transfers between devices, share(): return lax.all_to_all(copies, axis, split_axis=0, concat_axis=0, tiled=True)  50.7 us
    all_to_all x1, blocking collectives, per_device(): lax.all_to_all(gp.reshape((dp,) + proj_pair.shape), 'dp', split_axis=0, c...  31.5 us
    all_to_all x2, starting transfers between devices, share(): return lax.all_to_all(copies, axis, split_axis=0, concat_axis=0, tiled=True)  12.4 us
    unnamed x29, local copies, waits for them, and re-layouts  4.03 us
    broadcast_in_dim x2, local copies, waits for them, and re-layouts, share(): copies = jnp.broadcast_to(block[None], (count,) + block.shape)  3.5 us
  transfers between devices with their start and end apart: 2, of which 2 were waited for; matrix products, arithmetic and copies ran while one was open for 1% of the time, Pallas kernels for 0%

commit v1 on v0

v1 whole, which is shorter than its diff:
```python
import functools

import jax
import jax.numpy as jnp
from jax import lax
from jax.experimental import pallas as pl
from jax.experimental.pallas import tpu as pltpu
from jax.sharding import PartitionSpec as P

HEAD = 64
STATE = 128
LANES = 128
PAIR = 2 * STATE
EDGE = 16
NEXT = 8
exact = lax.Precision.HIGHEST
f32 = jnp.float32
bf16 = jnp.bfloat16

NN = (((1,), (0,)), ((), ()))
NT = (((1,), (1,)), ((), ()))
TN = (((0,), (0,)), ((), ()))


def mm(a, b, dims):
    return lax.dot_general(a, b, dims, preferred_element_type=f32)


def mm_exact(a, b, dims):
    return lax.dot_general(a, b, dims, precision=exact, preferred_element_type=f32)


def mm_split(a, b, dims):
    high = a.astype(bf16)
    low = (a - high.astype(f32)).astype(bf16)
    return mm(high, b, dims) + mm(low, b, dims)


def silu_parts(s):
    sig = jax.nn.sigmoid(s)
    return s * sig, sig * (1.0 + s * (1.0 - sig))


def mixer_kernel(
    sp,
    dp,
    heads,
    groups,
    chunks,
    normed_in,
    values_in,
    gate_in,
    up_in,
    proj_in,
    step,
    tap_v,
    tap_p,
    bias,
    log_rate,
    skip,
    gn,
    gv,
    gg,
    gs,
    gp,
    nrm,
    val,
    gate,
    up,
    proj,
    nt,
    ntall,
    cot,
    xvb,
    us,
    slv,
    upslope,
    xb,
    xeb,
    edy,
    dec,
    dgs,
    gm,
    pairx,
    bc,
    slp,
    ee,
    car,
    cin,
    cout,
    ybuf,
    dxl,
    zbuf,
    dvb,
    dpb,
    dpair,
    dpall,
    gpl,
    gin,
    gout,
    loc_sem,
    edge_sem,
    pj_send,
    pj_recv,
    pj_relay,
    ch_send,
    ch_recv,
    nx_sem,
    nt_send,
    nt_recv,
    dg_send,
    dg_recv,
    dg_relay,
    gc_send,
    gc_recv,
):
    z = lax.axis_index("sp")
    d = lax.axis_index("dp")
    T = cot.shape[0]
    W = cot.shape[1]
    width = nt.shape[0]
    R = proj_in.shape[0]
    GW = W // groups
    tiles = GW // LANES
    CW = GW // chunks
    nch = dp // 2
    core = lax.rem(d, 2)
    chip = d // 2
    sib = d + 1 - 2 * core
    first = z == 0
    last = z == sp - 1

    def remote(src, dst, ss, rs, to):
        return pltpu.make_async_remote_copy(
            src_ref=src,
            dst_ref=dst,
            send_sem=ss,
            recv_sem=rs,
            device_id=to,
            device_id_type=pl.DeviceIdType.MESH,
        )

    def prow(s):
        return pl.ds(pl.multiple_of(s * R, 16), R)

    def trow(s):
        return pl.ds(pl.multiple_of(s * T, LANES), T)

    def pcol(g):
        return slice(g * PAIR, (g + 1) * PAIR)

    below = lax.max(z - 1, 0)
    above = lax.min(z + 1, sp - 1)

    loads = [
        pltpu.make_async_copy(proj_in, proj.at[prow(d), :], loc_sem.at[0]),
        pltpu.make_async_copy(gate_in, gate, loc_sem.at[1]),
        pltpu.make_async_copy(up_in, up, loc_sem.at[2]),
        pltpu.make_async_copy(values_in, val.at[EDGE : EDGE + T, :], loc_sem.at[3]),
        pltpu.make_async_copy(normed_in, nrm.at[EDGE : EDGE + T, :], loc_sem.at[4]),
    ]
    for load in loads:
        load.start()

    barrier = pltpu.get_barrier_semaphore()
    for off in range(1, dp):
        pl.semaphore_signal(
            barrier,
            inc=1,
            device_id={"dp": lax.rem(d + off, dp)},
            device_id_type=pl.DeviceIdType.MESH,
        )

    @pl.when(z > 0)
    def _():
        pl.semaphore_signal(
            barrier, inc=1, device_id={"sp": below}, device_id_type=pl.DeviceIdType.MESH
        )

    @pl.when(z < sp - 1)
    def _():
        pl.semaphore_signal(
            barrier, inc=1, device_id={"sp": above}, device_id_type=pl.DeviceIdType.MESH
        )

    arrivals = dp - 1 + jnp.where(first, 0, 1) + jnp.where(last, 0, 1)
    pl.semaphore_wait(barrier, arrivals)

    def go_proj(g, s, to, ss):
        at = proj.at[prow(s), pcol(g)]
        return remote(at, at, ss, pj_recv.at[g, s], {"dp": to})

    def chip_peer(off):
        return lax.rem(chip + off, nch) * 2 + core

    def spread_out(go, send):
        for off in range(1, nch):
            to = chip_peer(off)
            go(d, to, send.at[to]).start()
        go(d, sib, send.at[sib]).start()

    def pass_on(go, send, relay):
        for off in range(1, nch):
            s = chip_peer(off)
            go(s, sib, relay.at[s]).wait_recv()
            go(s, sib, relay.at[s]).start()

    def take_rest(go, relay):
        go(sib, sib, relay.at[sib]).wait_recv()
        for off in range(1, nch):
            s = chip_peer(off) + 1 - 2 * core
            go(s, sib, relay.at[s]).wait_recv()

    def drain(go, send, relay):
        for off in range(1, nch):
            to = chip_peer(off)
            go(d, to, send.at[to]).wait_send()
            go(to, sib, relay.at[to]).wait_send()
        go(d, sib, send.at[sib]).wait_send()

    def proj_of(g):
        return lambda s, to, ss: go_proj(g, s, to, ss)

    loads[0].wait()
    spread_out(proj_of(0), pj_send.at[0])

    def go_edge(k):
        src = (values_in, normed_in)[k]
        dst = (val, nrm)[k]
        return remote(
            src.at[T - EDGE : T, :], dst.at[0:EDGE, :], edge_sem.at[0, k], edge_sem.at[1, k], {"sp": above}
        )

    @pl.when(z < sp - 1)
    def _():
        go_edge(0).start()
        go_edge(1).start()

    for g in range(1, groups):
        spread_out(proj_of(g), pj_send.at[g])

    @pl.when(first)
    def _():
        val[0:EDGE, :] = jnp.zeros((EDGE, W), bf16)
        nrm[0:EDGE, :] = jnp.zeros((EDGE, width), bf16)
        cin[0] = jnp.zeros((STATE, W), bf16)
        gin[0] = jnp.zeros(gin.shape[1:], bf16)

    @pl.when(last)
    def _():
        cin[1] = jnp.zeros((STATE, W), bf16)
        gin[1] = jnp.zeros(gin.shape[1:], bf16)
        dvb[:, T : T + NEXT, :] = jnp.zeros((dvb.shape[0], NEXT, LANES), f32)
        dpb[:, T : T + NEXT, :] = jnp.zeros((dpb.shape[0], NEXT, LANES), f32)

    row_i = lax.broadcasted_iota(jnp.int32, (T, T), 0)
    col_i = lax.broadcasted_iota(jnp.int32, (T, T), 1)
    causal = row_i >= col_i
    tri = causal.astype(f32)
    lane = lax.broadcasted_iota(jnp.int32, (T, LANES), 1)
    low = lane < HEAD

    def padded(v):
        return jnp.concatenate([v, jnp.zeros((v.shape[0], LANES - heads), f32)], axis=1)

    def spread(x, j):
        a = x[:, 2 * j : 2 * j + 1]
        b = x[:, 2 * j + 1 : 2 * j + 2]
        mask = low if x.shape[0] == T else low[0 : x.shape[0]]
        return jnp.where(mask, a, b)

    rate = -jnp.exp(padded(log_rate[...]))
    skips = padded(skip[...])
    steps = jnp.concatenate([step[...].astype(f32), jnp.zeros((LANES - heads, T), f32)], axis=0)
    raw = steps.T + padded(bias[...])
    dt = jax.nn.softplus(raw)
    sgs = jax.nn.sigmoid(raw)
    ac = mm_exact(tri, dt * rate, NN)
    ac_t = ac.T
    ea = jnp.exp(ac)
    end = ac[T - 1 : T, :]
    te = jnp.exp(end - ac)
    e_end = jnp.exp(end)

    def halves(v):
        zero = jnp.zeros_like(v)
        return jnp.concatenate([jnp.where(low, v, zero), jnp.where(low, zero, v)], axis=0)

    def conv(buf, k, taps, at):
        total = taps[0:1, at] * buf[k, EDGE - 3 : EDGE - 3 + T, :]
        for i in range(1, 4):
            total = total + taps[i : i + 1, at] * buf[k, EDGE - 3 + i : EDGE - 3 + i + T, :]
        return total

    def conv_back(buf, k, taps, at):
        total = taps[3:4, at] * buf[k, 0:T, :]
        for i in range(3):
            total = total + taps[i : i + 1, at] * buf[k, 3 - i : 3 - i + T, :]
        return total

    def before_pair(g):
        d_g = jnp.zeros((T, T), f32)
        for j in range(g * tiles, (g + 1) * tiles):
            at = slice(j * LANES, (j + 1) * LANES)
            v = gate[:, at].astype(f32)
            upf = up[:, at].astype(f32)
            act, slope = silu_parts(v)
            dy = (upf * act).astype(bf16)
            cot[:, at] = dy
            upslope[:, at] = upf * slope
            xvb[j] = val[:, at].astype(f32)
            u, slope = silu_parts(conv(xvb, j, tap_v, at))
            us[:, at] = u
            slv[:, at] = slope
            x = (u * spread(dt, j)).astype(bf16)
            xb[:, at] = x
            xeb[:, at] = (x.astype(f32) * spread(te, j)).astype(bf16)
            edy[:, at] = (spread(ea, j) * dy.astype(f32)).astype(bf16)
            ee[:, at] = spread(e_end, j)
            d_mix = mm(halves(dy), x, NT)
            for q in range(2):
                h = 2 * j + q
                diff = ac[:, h : h + 1] - ac_t[h : h + 1, :]
                decay = jnp.exp(jnp.where(causal, diff, -1e30))
                dec[h] = decay
                d_g = d_g + d_mix[q * T : (q + 1) * T] * decay
        dgs[g] = d_g.astype(bf16)

    def pair_stage(g):
        lanes = slice(g * GW, (g + 1) * GW)
        pb = mm(nrm[...], proj[:, pcol(g)], NN).astype(bf16).astype(f32)
        for i in range(2):
            k = 2 * g + i
            at = slice(k * LANES, (k + 1) * LANES)
            pairx[k] = pb[:, i * LANES : (i + 1) * LANES]
            act, slope = silu_parts(conv(pairx, k, tap_p, at))
            bc[k] = act.astype(bf16)
            slp[k] = slope
        b = bc[2 * g]
        cc = bc[2 * g + 1]
        gm[g] = mm(cc, b, NT)
        car[0, :, lanes] = mm(b, xeb[:, lanes], TN)
        car[1, :, lanes] = mm(cc, edy[:, lanes], TN)

    def local_mix(g):
        gmat = gm[g]
        for j in range(g * tiles, (g + 1) * tiles):
            at = slice(j * LANES, (j + 1) * LANES)
            mixes = [(gmat * dec[2 * j + q]).astype(bf16) for q in range(2)]
            ybuf[:, at] = mm(jnp.concatenate(mixes, axis=1), halves(xb[:, at]), NN)
            dxl[:, at] = mm(jnp.concatenate(mixes, axis=0), halves(cot[:, at]), TN)

    def has_in(q):
        return jnp.where(q == 0, z > 0, z < sp - 1)

    def has_out(q):
        return jnp.where(q == 0, z < sp - 1, z > 0)

    def onward(q):
        return lax.max(lax.min(z + 1 - 2 * q, sp - 1), 0)

    def go_state(q, i):
        lanes = slice(i * CW, (i + 1) * CW)
        return remote(
            cout.at[q, :, lanes], cin.at[q, :, lanes], ch_send.at[q, i], ch_recv.at[q, i], {"sp": onward(q)}
        )

    def chain(q, g):
        for i in range(g * chunks, (g + 1) * chunks):
            lanes = slice(i * CW, (i + 1) * CW)

            @pl.when(has_in(q))
            def _():
                go_state(q, i).wait_recv()

            @pl.when(has_out(q))
            def _():
                total = cin[q, :, lanes].astype(f32) * ee[0:1, lanes] + car[q, :, lanes]
                cout[q, :, lanes] = total.astype(bf16)
                go_state(q, i).start()

    early = jnp.where(z < sp // 2, 0, 1)
    late = 1 - early
    at_end = (z == 0) | (z == sp - 1)

    def go_next(kind, g):
        buf = (dpb, dvb)[kind]
        n = (2, tiles)[kind]
        part = buf.at[g * n : (g + 1) * n]
        return remote(
            part.at[:, 0:NEXT, :],
            part.at[:, T : T + NEXT, :],
            nx_sem.at[0, kind, g],
            nx_sem.at[1, kind, g],
            {"sp": below},
        )

    def send_next(kind, g):
        @pl.when(z > 0)
        def _():
            go_next(kind, g).start()

    def take_next(kind, g):
        @pl.when(z < sp - 1)
        def _():
            go_next(kind, g).wait_recv()

    def pair_grads(g):
        lanes = slice(g * GW, (g + 1) * GW)
        b = bc[2 * g]
        cc = bc[2 * g + 1]
        dg = dgs[g]
        d_b = mm(dg, cc, TN) + mm(xeb[:, lanes], cin[1, :, lanes], NT)
        d_c = mm(dg, b, NN) + mm(edy[:, lanes], cin[0, :, lanes], NT)
        dpb[2 * g, 0:T, :] = d_b * slp[2 * g]
        dpb[2 * g + 1, 0:T, :] = d_c * slp[2 * g + 1]
        send_next(0, g)

    def go_dpair(g):
        def go(s, to, ss):
            at = dpall.at[trow(s), pcol(g)]
            return remote(at, at, ss, dg_recv.at[g, s], {"dp": to})

        return go

    def pair_back(g):
        take_next(0, g)
        for i in range(2):
            k = 2 * g + i
            at = slice(k * LANES, (k + 1) * LANES)
            grad = conv_back(dpb, k, tap_p, at).astype(bf16)
            dpair[:, at] = grad
            dpall[trow(d), at] = grad
        spread_out(go_dpair(g), dg_send.at[g])

    def value_grads(g):
        b = bc[2 * g]
        cc = bc[2 * g + 1]
        for j in range(g * tiles, (g + 1) * tiles):
            at = slice(j * LANES, (j + 1) * LANES)
            s_in = cin[0, :, at]
            ds = cin[1, :, at]
            dyf = cot[:, at].astype(f32)
            u = us[:, at]
            y = ybuf[:, at] + spread(ea, j) * mm(cc, s_in, NN)
            zbuf[0, 0:T, at] = dyf * y
            ybf = (y + spread(skips, j) * u).astype(bf16)
            gg[:, at] = (upslope[:, at] * ybf.astype(f32)).astype(bf16)
            x = xb[:, at].astype(f32)
            tej = spread(te, j)
            far = mm(b, ds, NN)
            dx = dxl[:, at] + tej * far
            zbuf[1, 0:T, at] = x * dx
            ends = jnp.sum(x * tej * far, axis=0, keepdims=True) + ee[:, at] * jnp.sum(
                ds.astype(f32) * s_in.astype(f32), axis=0, keepdims=True
            )
            zbuf[1, T : T + NEXT, at] = jnp.broadcast_to(ends, (NEXT, LANES))
            du = spread(dt, j) * dx + spread(skips, j) * dyf
            dvb[j, 0:T, :] = du * slv[:, at]
        send_next(1, g)

    def value_back(g):
        take_next(1, g)
        for j in range(g * tiles, (g + 1) * tiles):
            at = slice(j * LANES, (j + 1) * LANES)
            gv[:, at] = conv_back(dvb, j, tap_v, at).astype(bf16)

    def step_grads():
        sel_r = lax.broadcasted_iota(jnp.int32, (LANES, W), 0)
        sel_c = lax.broadcasted_iota(jnp.int32, (LANES, W), 1)
        sel = jnp.where(sel_c // HEAD == sel_r, 1.0, 0.0).astype(bf16)
        r1 = mm_split(zbuf[0, 0:T, :], sel, NT)
        both = mm_split(zbuf[1], sel, NT)
        xd = both[0:T]
        d_end = both[T : T + 1]
        back = mm_exact(tri, r1 - xd, TN) + d_end
        d_dt = (xd / dt + rate * back) * sgs
        gs[...] = d_dt.T[0:heads, :].astype(bf16)

    def go_nt(to):
        return remote(
            nt.at[prow(to), :], ntall.at[:, trow(d)], nt_send.at[to], nt_recv.at[d], {"dp": to}
        )

    def nt_from(s):
        return remote(nt.at[prow(d), :], ntall.at[:, trow(s)], nt_send.at[s], nt_recv.at[s], {"dp": s})

    def send_normed():
        for k in range(width // LANES):
            at = slice(k * LANES, (k + 1) * LANES)
            nt[at, :] = nrm[EDGE : EDGE + T, at].T
        for off in range(1, dp):
            go_nt(lax.rem(d + off, dp)).start()
        ntall[:, trow(d)] = nt[prow(d), :]

    def go_rows(q, k):
        lanes = slice(k * LANES, (k + 1) * LANES)
        return remote(
            gout.at[q, :, lanes], gin.at[q, :, lanes], gc_send.at[q, k], gc_recv.at[q, k], {"sp": onward(q)}
        )

    def rows_step(q, k):
        lanes = slice(k * LANES, (k + 1) * LANES)

        @pl.when(has_in(q))
        def _():
            go_rows(q, k).wait_recv()

        @pl.when(has_out(q))
        def _():
            gout[q, :, lanes] = (gin[q, :, lanes].astype(f32) + gpl[:, lanes]).astype(bf16)
            go_rows(q, k).start()

    def rows_product(g):
        take_rest(go_dpair(g), dg_relay.at[g])
        gpl[:, pcol(g)] = mm(ntall[...], dpall[:, pcol(g)], NN)

    def rows_total(k):
        lanes = slice(k * LANES, (k + 1) * LANES)
        gp[:, lanes] = gin[0, :, lanes].astype(f32) + gpl[:, lanes] + gin[1, :, lanes].astype(f32)

    loads[1].wait()
    loads[2].wait()
    loads[3].wait()

    @pl.when(z > 0)
    def _():
        go_edge(0).wait_recv()

    before_pair(0)
    pass_on(proj_of(0), pj_send.at[0], pj_relay.at[0])
    for g in range(1, groups):
        before_pair(g)
    loads[4].wait()

    @pl.when(z > 0)
    def _():
        go_edge(1).wait_recv()

    for g in range(groups):
        if g > 0:
            pass_on(proj_of(g), pj_send.at[g], pj_relay.at[g])
        take_rest(proj_of(g), pj_relay.at[g])
        pair_stage(g)

        @pl.when(at_end)
        def _():
            chain(early, g)

        local_mix(g)
        if g == 0:
            send_normed()

    for g in range(groups):
        @pl.when(jnp.logical_not(at_end))
        def _():
            chain(early, g)

        chain(late, g)
        pair_grads(g)
        if g > 0:
            value_grads(g - 1)
        pair_back(g)
    value_grads(groups - 1)
    for g in range(groups):
        pass_on(go_dpair(g), dg_send.at[g], dg_relay.at[g])
    for s in range(1, dp):
        nt_from(lax.rem(d + s, dp)).wait_recv()
    for g in range(groups):
        rows_product(g)
        for k in range(2 * g, 2 * g + 2):
            @pl.when(at_end)
            def _():
                rows_step(early, k)

    for k in range(2 * groups):
        @pl.when(jnp.logical_not(at_end))
        def _():
            rows_step(early, k)

    for k in range(width // 512):
        at = slice(k * 512, (k + 1) * 512)
        gn[:, at] = mm(dpair[...], proj[at, :], NT).astype(bf16)
    for g in range(groups):
        value_back(g)
    step_grads()
    for k in range(2 * groups):
        rows_step(late, k)
        rows_total(k)

    for g in range(groups):
        drain(proj_of(g), pj_send.at[g], pj_relay.at[g])
        drain(go_dpair(g), dg_send.at[g], dg_relay.at[g])
    for off in range(1, dp):
        go_nt(lax.rem(d + off, dp)).wait_send()

    @pl.when(z < sp - 1)
    def _():
        go_edge(0).wait_send()
        go_edge(1).wait_send()

    @pl.when(z > 0)
    def _():
        for g in range(groups):
            go_next(0, g).wait_send()
            go_next(1, g).wait_send()

    for q in range(2):
        @pl.when(has_out(q))
        def _():
            for i in range(groups * chunks):
                go_state(q, i).wait_send()
            for k in range(2 * groups):
                go_rows(q, k).wait_send()


def per_device(
    normed,
    values,
    gate_in,
    step_raw,
    upstream,
    proj_pair,
    conv_value,
    conv_pair,
    step_bias,
    decay_log,
    skip,
):
    sp = lax.axis_size("sp")
    dp = lax.axis_size("dp")
    T = normed.shape[1]
    width = normed.shape[2]
    W = values.shape[2]
    heads = step_raw.shape[2]
    cols = proj_pair.shape[1]
    groups = cols // PAIR
    R = proj_pair.shape[0]
    chunks = 4
    vmem = pl.BlockSpec(memory_space=pltpu.VMEM)
    anyspace = pl.BlockSpec(memory_space=pl.ANY)
    V = pltpu.VMEM
    dma = pltpu.SemaphoreType.DMA
    vt = W // LANES
    pt = cols // LANES
    scratch = [
        V((EDGE + T, width), bf16),
        V((EDGE + T, W), bf16),
        V((T, W), bf16),
        V((T, W), bf16),
        V((width, cols), bf16),
        V((width, T), bf16),
        V((R, dp * T), bf16),
        V((T, W), bf16),
        V((vt, EDGE + T, LANES), f32),
        V((T, W), f32),
        V((T, W), f32),
        V((T, W), f32),
        V((T, W), bf16),
        V((T, W), bf16),
        V((T, W), bf16),
        V((heads, T, T), f32),
        V((groups, T, T), bf16),
        V((groups, T, T), f32),
        V((pt, EDGE + T, LANES), f32),
        V((pt, T, LANES), bf16),
        V((pt, T, LANES), f32),
        V((1, W), f32),
        V((2, STATE, W), f32),
        V((2, STATE, W), bf16),
        V((2, STATE, W), bf16),
        V((T, W), f32),
        V((T, W), f32),
        V((2, T + NEXT, W), f32),
        V((vt, T + NEXT, LANES), f32),
        V((pt, T + NEXT, LANES), f32),
        V((T, cols), bf16),
        V((dp * T, cols), bf16),
        V((R, cols), f32),
        V((2, R, cols), bf16),
        V((2, R, cols), bf16),
        dma((5,)),
        dma((2, 2)),
        dma((groups, dp)),
        dma((groups, dp)),
        dma((groups, dp)),
        dma((2, groups * chunks)),
        dma((2, groups * chunks)),
        dma((2, 2, groups)),
        dma((dp,)),
        dma((dp,)),
        dma((groups, dp)),
        dma((groups, dp)),
        dma((groups, dp)),
        dma((2, pt)),
        dma((2, pt)),
    ]
    gn, gv, gg, gs, gp = pl.pallas_call(
        functools.partial(mixer_kernel, sp, dp, heads, groups, chunks),
        out_shape=(
            jax.ShapeDtypeStruct((T, width), bf16),
            jax.ShapeDtypeStruct((T, W), bf16),
            jax.ShapeDtypeStruct((T, W), bf16),
            jax.ShapeDtypeStruct((heads, T), bf16),
            jax.ShapeDtypeStruct((R, cols), f32),
        ),
        in_specs=[anyspace] * 5 + [vmem] * 6,
        out_specs=(vmem,) * 5,
        scratch_shapes=scratch,
        compiler_params=pltpu.CompilerParams(
            collective_id=0, has_side_effects=True, vmem_limit_bytes=56 * 1024 * 1024
        ),
    )(
        normed[0],
        values[0],
        gate_in[0],
        upstream[0],
        proj_pair,
        step_raw[0].T,
        conv_value,
        conv_pair,
        step_bias[None],
        decay_log[None],
        skip[None],
    )
    return (gn[None], gv[None], gg[None], gs.T[None], gp)


def solution(mesh):
    tok = P("dp", "sp", None)
    in_specs = (tok, tok, tok, tok, tok, P("dp", None), P(), P(), P(), P(), P())
    out_specs = (tok, tok, tok, tok, P("dp", None))
    return jax.shard_map(
        per_device, mesh=mesh, in_specs=in_specs, out_specs=out_specs, check_vma=False
    )
```

time: 172 us -> 77.6 us (0.45)
  waiting for transfers between devices: 50.7 us -> 0 us
  blocking collectives: 31.5 us -> 0 us
  starting transfers between devices: 12.4 us -> 0 us
  Pallas kernels: 67.5 us -> 71.3 us
  local copies, waits for them, and re-layouts: 7.8 us -> 5.36 us
    all_to_all x2 -> x0, waiting for transfers between devices: 50.7 us -> none  [share(): return lax.all_to_all(copies, axis, split_axis=0, concat_axis=0, tiled=True)]
    all_to_all x1 -> x0, blocking collectives: 31.5 us -> none  [per_device(): lax.all_to_all(gp.reshape((dp,) + proj_pair.shape), 'dp', split_axis=0, c...]
    all_to_all x2 -> x0, starting transfers between devices: 12.4 us -> none  [share(): return lax.all_to_all(copies, axis, split_axis=0, concat_axis=0, tiled=True)]
    pallas_call x1, Pallas kernels: 67.5 us -> 71.3 us  [per_device(): pl.pallas_call(functools.partial(mixer_kernel, sp, dp, heads, groups, chu...]
    broadcast_in_dim x5 -> x0, local copies, waits for them, and re-layouts: 3.51 us -> none  [the longest x2 3.5 us: share(): copies = jnp.broadcast_to(block[None], (count,) + block.shape)]
    unnamed x29 -> x13, local copies, waits for them, and re-layouts: 4.03 us -> 5.36 us
  transfers between devices with their start and end apart: 2 -> 0, of which waited for: 2 -> 0; matrix products, arithmetic and copies ran while one was open for 1% -> 0% of each run, Pallas kernels for 0% -> 0%
where the time goes in v1:
time: 77.6 us; the launch traced here: 77.4 us
  Pallas kernels  71.3 us (92%)
  local copies, waits for them, and re-layouts  5.36 us (7%)
    pallas_call x1, Pallas kernels, per_device(): pl.pallas_call(functools.partial(mixer_kernel, sp, dp, heads, groups, chu...  71.3 us
    unnamed x13, local copies, waits for them, and re-layouts  5.36 us

profile of v1, /device:TPU:0, one launch (start us, length us, event | category | flops | bytes accessed | tf_op | source)
XLA Modules:
  0.0 77.4 jit_solution(9094090425015434175)
XLA Ops:
  0.6 71.3 %shard_map.146 = (bf16[128,2048]{1,0:T(8,128)(2,1)}, bf16[128,2048]{1,0:T(8,128)(2,1)}, bf16[128,2048]{1,0:T(8,128)(2,1)}, bf16[32,128]{1,0:T(8,128)(2,1)}, f32[256,512]{1,0:T(8,128)}) custom-call(bf16[128,2048]{1,0:T(8,128)(2,1)} %bitcast.16, bf16[128,2048]{1,0:T(8,128)(2,1)} %bitcast.17, bf16[128,2048]{1,0:T(8,128)(2,1)} %bitcast.18, ...), custom_call_target="tpu_custom_call" | custom-call | tf_op jit(solution)/shard_map/pallas_call | solution.py:698
  72.0 0.0 copy-start.2
  72.0 1.9 %copy.21 = bf16[1,128,2048]{2,1,0:T(8,128)(2,1)} copy(bf16[1,128,2048]{2,1,0:T(8,128)(2,1)} %bitcast.22) | data formatting | bytes 1048576
  73.9 0.0 copy-done.2
  73.9 0.0 copy-start.1
  73.9 0.8 %copy.22 = bf16[1,128,2048]{2,1,0:T(8,128)(2,1)} copy(bf16[1,128,2048]{2,1,0:T(8,128)(2,1)S(1)} %bitcast.21) | data formatting | bytes 1048576
  74.7 0.4 copy-done.1
  75.2 0.0 copy-start.3
  75.2 0.0 copy-start
  75.2 0.8 %copy.23 = bf16[1,128,2048]{2,1,0:T(8,128)(2,1)} copy(bf16[1,128,2048]{2,1,0:T(8,128)(2,1)S(1)} %bitcast.20) | data formatting | bytes 1048576
  76.0 0.0 copy-done.3
  76.0 0.6 copy.24
  76.6 0.0 copy-done
  76.6 0.8 %copy.25 = f32[256,512]{1,0:T(8,128)} copy(f32[256,512]{1,0:T(8,128)S(1)} %copy-done) | data formatting | bytes 1048576
Async XLA Ops:
  72.0 2.0 %copy-start.2 = (bf16[128,2048]{1,0:T(8,128)(2,1)S(1)}, bf16[128,2048]{1,0:T(8,128)(2,1)}, u32[]{:S(2)}) copy-start(bf16[128,2048]{1,0:T(8,128)(2,1)} %get-tuple-element.11) | copy-start | bytes 1572868
  73.9 1.2 %copy-start.1 = (bf16[128,2048]{1,0:T(8,128)(2,1)S(1)}, bf16[128,2048]{1,0:T(8,128)(2,1)}, u32[]{:S(2)}) copy-start(bf16[128,2048]{1,0:T(8,128)(2,1)} %get-tuple-element.12) | copy-start | bytes 1572868
  75.2 0.8 %copy-start.3 = (bf16[32,128]{1,0:T(8,128)(2,1)S(1)}, bf16[32,128]{1,0:T(8,128)(2,1)}, u32[]{:S(2)}) copy-start(bf16[32,128]{1,0:T(8,128)(2,1)} %get-tuple-element.13) | copy-start | bytes 24580
  75.2 1.4 %copy-start = (f32[256,512]{1,0:T(8,128)S(1)}, f32[256,512]{1,0:T(8,128)}, u32[]{:S(2)}) copy-start(f32[256,512]{1,0:T(8,128)} %get-tuple-element.24) | copy-start | bytes 1572868

commit v2 on v1

--- a/solution.py
+++ b/solution.py
@@ -47,22 +47,29 @@
     heads,
     groups,
     chunks,
+    cuts,
     normed_in,
     values_in,
     gate_in,
     up_in,
     proj_in,
+    step_in,
+    tap_v_in,
+    tap_p_in,
+    bias_in,
+    log_rate_in,
+    skip_in,
+    gn,
+    gv,
+    gg,
+    gs,
+    gp,
     step,
     tap_v,
     tap_p,
     bias,
     log_rate,
     skip,
-    gn,
-    gv,
-    gg,
-    gs,
-    gp,
     nrm,
     val,
     gate,
@@ -159,7 +166,21 @@
         pltpu.make_async_copy(values_in, val.at[EDGE : EDGE + T, :], loc_sem.at[3]),
         pltpu.make_async_copy(normed_in, nrm.at[EDGE : EDGE + T, :], loc_sem.at[4]),
     ]
-    for load in loads:
+    small = [
+        pltpu.make_async_copy(src, dst, loc_sem.at[5 + k])
+        for k, (src, dst) in enumerate(
+            (
+                (step_in, step),
+                (bias_in, bias),
+                (log_rate_in, log_rate),
+                (skip_in, skip),
+                (tap_v_in, tap_v),
+                (tap_p_in, tap_p),
+            )
+        )
+    ]
+    loads[0].start()
+    for load in small + loads[1:]:
         load.start()
 
     barrier = pltpu.get_barrier_semaphore()
@@ -253,6 +274,8 @@
         dvb[:, T : T + NEXT, :] = jnp.zeros((dvb.shape[0], NEXT, LANES), f32)
         dpb[:, T : T + NEXT, :] = jnp.zeros((dpb.shape[0], NEXT, LANES), f32)
 
+    for load in small:
+        load.wait()
     row_i = lax.broadcasted_iota(jnp.int32, (T, T), 0)
     col_i = lax.broadcasted_iota(jnp.int32, (T, T), 1)
     causal = row_i >= col_i
@@ -365,19 +388,29 @@
             cout.at[q, :, lanes], cin.at[q, :, lanes], ch_send.at[q, i], ch_recv.at[q, i], {"sp": onward(q)}
         )
 
-    def chain(q, g):
-        for i in range(g * chunks, (g + 1) * chunks):
-            lanes = slice(i * CW, (i + 1) * CW)
-
-            @pl.when(has_in(q))
-            def _():
-                go_state(q, i).wait_recv()
-
-            @pl.when(has_out(q))
-            def _():
-                total = cin[q, :, lanes].astype(f32) * ee[0:1, lanes] + car[q, :, lanes]
-                cout[q, :, lanes] = total.astype(bf16)
-                go_state(q, i).start()
+    def chain_step(q, i):
+        lanes = slice(i * CW, (i + 1) * CW)
+
+        @pl.when(has_in(q))
+        def _():
+            go_state(q, i).wait_recv()
+
+        @pl.when(has_out(q))
+        def _():
+            total = cin[q, :, lanes].astype(f32) * ee[0:1, lanes] + car[q, :, lanes]
+            cout[q, :, lanes] = total.astype(bf16)
+            go_state(q, i).start()
+
+    def chain_ends(g):
+        @pl.when(at_end)
+        def _():
+            for i in range(g * chunks, (g + 1) * chunks):
+                chain_step(early, i)
+
+    def chain_early(i):
+        @pl.when(jnp.logical_not(at_end))
+        def _():
+            chain_step(early, i)
 
     early = jnp.where(z < sp // 2, 0, 1)
     late = 1 - early
@@ -493,14 +526,18 @@
             go_nt(lax.rem(d + off, dp)).start()
         ntall[:, trow(d)] = nt[prow(d), :]
 
+    def row_part(k):
+        g, i = divmod(k, cuts)
+        return slice(i * (R // cuts), (i + 1) * (R // cuts)), pcol(g)
+
     def go_rows(q, k):
-        lanes = slice(k * LANES, (k + 1) * LANES)
+        r, c = row_part(k)
         return remote(
-            gout.at[q, :, lanes], gin.at[q, :, lanes], gc_send.at[q, k], gc_recv.at[q, k], {"sp": onward(q)}
+            gout.at[q, r, c], gin.at[q, r, c], gc_send.at[q, k], gc_recv.at[q, k], {"sp": onward(q)}
         )
 
     def rows_step(q, k):
-        lanes = slice(k * LANES, (k + 1) * LANES)
+        r, c = row_part(k)
 
         @pl.when(has_in(q))
         def _():
@@ -508,16 +545,31 @@
 
         @pl.when(has_out(q))
         def _():
-            gout[q, :, lanes] = (gin[q, :, lanes].astype(f32) + gpl[:, lanes]).astype(bf16)
+            gout[q, r, c] = (gin[q, r, c].astype(f32) + gpl[r, c]).astype(bf16)
             go_rows(q, k).start()
+
+    def rows_ends(g):
+        @pl.when(at_end)
+        def _():
+            for k in range(g * cuts, (g + 1) * cuts):
+                rows_step(early, k)
+
+    def rows_early(k):
+        @pl.when(jnp.logical_not(at_end))
+        def _():
+            rows_step(early, k)
 
     def rows_product(g):
         take_rest(go_dpair(g), dg_relay.at[g])
         gpl[:, pcol(g)] = mm(ntall[...], dpall[:, pcol(g)], NN)
 
     def rows_total(k):
-        lanes = slice(k * LANES, (k + 1) * LANES)
-        gp[:, lanes] = gin[0, :, lanes].astype(f32) + gpl[:, lanes] + gin[1, :, lanes].astype(f32)
+        r, c = row_part(k)
+        gp[r, c] = gin[0, r, c].astype(f32) + gpl[r, c] + gin[1, r, c].astype(f32)
+
+    def pass_proj(g):
+        pass_on(proj_of(g), pj_send.at[g], pj_relay.at[g])
+        take_rest(proj_of(g), pj_relay.at[g])
 
     loads[1].wait()
     loads[2].wait()
@@ -527,9 +579,7 @@
     def _():
         go_edge(0).wait_recv()
 
-    before_pair(0)
-    pass_on(proj_of(0), pj_send.at[0], pj_relay.at[0])
-    for g in range(1, groups):
+    for g in range(groups):
         before_pair(g)
     loads[4].wait()
 
@@ -537,54 +587,56 @@
     def _():
         go_edge(1).wait_recv()
 
-    for g in range(groups):
-        if g > 0:
-            pass_on(proj_of(g), pj_send.at[g], pj_relay.at[g])
+    pass_proj(0)
+    pair_stage(0)
+    chain_ends(0)
+    local_mix(0)
+    send_normed()
+    done_early = 0
+    for g in range(1, groups):
+        pass_on(proj_of(g), pj_send.at[g], pj_relay.at[g])
+        for _ in range(chunks // 4):
+            chain_early(done_early)
+            done_early += 1
         take_rest(proj_of(g), pj_relay.at[g])
         pair_stage(g)
-
-        @pl.when(at_end)
-        def _():
-            chain(early, g)
-
-        local_mix(g)
-        if g == 0:
-            send_normed()
-
-    for g in range(groups):
-        @pl.when(jnp.logical_not(at_end))
-        def _():
-            chain(early, g)
-
-        chain(late, g)
-        pair_grads(g)
-        if g > 0:
-            value_grads(g - 1)
-        pair_back(g)
-    value_grads(groups - 1)
+        chain_ends(g)
+
+    order = [(i, 0, i) for i in range(done_early, groups * chunks)]
+    order += [(i + chunks // 2 + 0.5, 1, i) for i in range(groups * chunks)]
+    for _, kind, i in sorted(order):
+        if kind == 0:
+            chain_early(i)
+            continue
+        chain_step(late, i)
+        if (i + 1) % chunks == 0:
+            g = i // chunks
+            pair_grads(g)
+            pair_back(g)
+            if g + 1 < groups:
+                local_mix(g + 1)
+
+    for s in range(1, dp):
+        nt_from(lax.rem(d + s, dp)).wait_recv()
+    sent = 0
     for g in range(groups):
         pass_on(go_dpair(g), dg_send.at[g], dg_relay.at[g])
-    for s in range(1, dp):
-        nt_from(lax.rem(d + s, dp)).wait_recv()
-    for g in range(groups):
+        while sent < g * cuts:
+            rows_early(sent)
+            sent += 1
         rows_product(g)
-        for k in range(2 * g, 2 * g + 2):
-            @pl.when(at_end)
-            def _():
-                rows_step(early, k)
-
-    for k in range(2 * groups):
-        @pl.when(jnp.logical_not(at_end))
-        def _():
-            rows_step(early, k)
-
+        rows_ends(g)
+        value_grads(g)
     for k in range(width // 512):
         at = slice(k * 512, (k + 1) * 512)
         gn[:, at] = mm(dpair[...], proj[at, :], NT).astype(bf16)
+    while sent < groups * cuts:
+        rows_early(sent)
+        sent += 1
     for g in range(groups):
         value_back(g)
     step_grads()
-    for k in range(2 * groups):
+    for k in range(groups * cuts):
         rows_step(late, k)
         rows_total(k)
 
@@ -610,8 +662,17 @@
         def _():
             for i in range(groups * chunks):
                 go_state(q, i).wait_send()
-            for k in range(2 * groups):
+            for k in range(groups * cuts):
                 go_rows(q, k).wait_send()
+
+
+def place_kernel(*refs):
+    sources, targets, sem = refs[0:5], refs[5:10], refs[10]
+    copies = [pltpu.make_async_copy(sources[k], targets[k], sem.at[k]) for k in range(5)]
+    for copy in copies:
+        copy.start()
+    for copy in copies:
+        copy.wait()
 
 
 def per_device(
@@ -636,14 +697,21 @@
     cols = proj_pair.shape[1]
     groups = cols // PAIR
     R = proj_pair.shape[0]
-    chunks = 4
+    chunks = min(8, W // groups // LANES)
+    cuts = 4
     vmem = pl.BlockSpec(memory_space=pltpu.VMEM)
-    anyspace = pl.BlockSpec(memory_space=pl.ANY)
+    hbm = pl.BlockSpec(memory_space=pltpu.HBM)
     V = pltpu.VMEM
     dma = pltpu.SemaphoreType.DMA
     vt = W // LANES
     pt = cols // LANES
     scratch = [
+        V((heads, T), bf16),
+        V((4, W), f32),
+        V((4, cols), f32),
+        V((1, heads), f32),
+        V((1, heads), f32),
+        V((1, heads), f32),
         V((EDGE + T, width), bf16),
         V((EDGE + T, W), bf16),
         V((T, W), bf16),
@@ -679,7 +747,7 @@
         V((R, cols), f32),
         V((2, R, cols), bf16),
         V((2, R, cols), bf16),
-        dma((5,)),
+        dma((11,)),
         dma((2, 2)),
         dma((groups, dp)),
         dma((groups, dp)),
@@ -692,11 +760,11 @@
         dma((groups, dp)),
         dma((groups, dp)),
         dma((groups, dp)),
-        dma((2, pt)),
-        dma((2, pt)),
+        dma((2, groups * cuts)),
+        dma((2, groups * cuts)),
     ]
     gn, gv, gg, gs, gp = pl.pallas_call(
-        functools.partial(mixer_kernel, sp, dp, heads, groups, chunks),
+        functools.partial(mixer_kernel, sp, dp, heads, groups, chunks, cuts),
         out_shape=(
             jax.ShapeDtypeStruct((T, width), bf16),
             jax.ShapeDtypeStruct((T, W), bf16),
@@ -704,25 +772,39 @@
             jax.ShapeDtypeStruct((heads, T), bf16),
             jax.ShapeDtypeStruct((R, cols), f32),
         ),
-        in_specs=[anyspace] * 5 + [vmem] * 6,
+        in_specs=[hbm] * 11,
         out_specs=(vmem,) * 5,
         scratch_shapes=scratch,
         compiler_params=pltpu.CompilerParams(
-            collective_id=0, has_side_effects=True, vmem_limit_bytes=56 * 1024 * 1024
+            collective_id=0, has_side_effects=True, vmem_limit_bytes=40 * 1024 * 1024
         ),
     )(
-        normed[0],
-        values[0],
-        gate_in[0],
-        upstream[0],
-        proj_pair,
-        step_raw[0].T,
-        conv_value,
-        conv_pair,
-        step_bias[None],
-        decay_log[None],
-        skip[None],
+        *[
+            pltpu.with_memory_space_constraint(x, pltpu.HBM)
+            for x in (
+                normed[0],
+                values[0],
+                gate_in[0],
+                upstream[0],
+                proj_pair,
+                step_raw[0].T,
+                conv_value,
+                conv_pair,
+                step_bias[None],
+                decay_log[None],
+                skip[None],
+            )
+        ]
     )
+    results = (gn, gv, gg, gs, gp)
+    gn, gv, gg, gs, gp = pl.pallas_call(
+        place_kernel,
+        out_shape=tuple(jax.ShapeDtypeStruct(r.shape, r.dtype) for r in results),
+        in_specs=[vmem] * 5,
+        out_specs=(hbm,) * 5,
+        scratch_shapes=[dma((5,))],
+        compiler_params=pltpu.CompilerParams(vmem_limit_bytes=8 * 1024 * 1024),
+    )(*results)
     return (gn[None], gv[None], gg[None], gs.T[None], gp)
 
 

time: 77.6 us -> 64.5 us (0.83)
  Pallas kernels: 71.3 us -> 63.7 us
  local copies, waits for them, and re-layouts: 5.36 us -> 0 us
    pallas_call x1, Pallas kernels: 71.3 us -> 62.4 us  [per_device(): pl.pallas_call(functools.partial(mixer_kernel, sp, dp, heads, groups, chu...]
    unnamed x13 -> x0, local copies, waits for them, and re-layouts: 5.36 us -> none
    pallas_call x0 -> x1, Pallas kernels: none -> 1.36 us  [per_device(): pl.pallas_call(place_kernel, out_shape=tuple((jax.ShapeDtypeStruct(r.shap...]
where the time goes in v2:
time: 64.5 us; the launch traced here: 64.4 us
  Pallas kernels  63.7 us (99%)
    pallas_call x1, Pallas kernels, per_device(): pl.pallas_call(functools.partial(mixer_kernel, sp, dp, heads, groups, chu...  62.4 us
    pallas_call x1, Pallas kernels, per_device(): pl.pallas_call(place_kernel, out_shape=tuple((jax.ShapeDtypeStruct(r.shap...  1.36 us

profile of v2, /device:TPU:0, one launch (start us, length us, event | category | flops | bytes accessed | tf_op | source)
XLA Modules:
  0.0 64.4 jit_solution(12137498935676639094)
XLA Ops:
  0.6 62.4 %shard_map.146 = (bf16[128,2048]{1,0:T(8,128)(2,1)S(1)}, bf16[128,2048]{1,0:T(8,128)(2,1)S(1)}, bf16[128,2048]{1,0:T(8,128)(2,1)S(1)}, bf16[32,128]{1,0:T(8,128)(2,1)S(1)}, f32[256,512]{1,0:T(8,128)S(1)}) custom-call(bf16[128,2048]{1,0:T(8,128)(2,1)} %bitcast.16, bf16[128,2048]{1,0:T(8,128)(2,1)} %bitcast.17, bf16[128,2048]{1,0:T(8,128)(2,1)} %bitcast.18, ...), custom_call_target="tpu_custom_call" | custom-call | tf_op jit(solution)/shard_map/pallas_call | solution.py:766
  63.0 1.4 %shard_map.147 = (bf16[128,2048]{1,0:T(8,128)(2,1)}, bf16[128,2048]{1,0:T(8,128)(2,1)}, bf16[128,2048]{1,0:T(8,128)(2,1)}, bf16[32,128]{1,0:T(8,128)(2,1)}, f32[256,512]{1,0:T(8,128)}) custom-call(bf16[128,2048]{1,0:T(8,128)(2,1)S(1)} %get-tuple-element.15.refs_0_, bf16[128,2048]{1,0:T(8,128)(2,1)S(1)} %get-tuple-element.16.refs_1_, ...), custom_call_target="tpu_custom_call" | custom-call | tf_op jit(solution)/shard_map/pallas_call | solution.py:800

commit v3 on v2

--- a/solution.py
+++ b/solution.py
@@ -100,6 +100,7 @@
     zbuf,
     dvb,
     dpb,
+    dpn,
     dpair,
     dpall,
     gpl,
@@ -150,8 +151,11 @@
     def prow(s):
         return pl.ds(pl.multiple_of(s * R, 16), R)
 
-    def trow(s):
-        return pl.ds(pl.multiple_of(s * T, LANES), T)
+    def twice(s):
+        return pl.ds(pl.multiple_of(s * 2 * T, LANES), 2 * T)
+
+    def sent_rows(s):
+        return pl.ds(pl.multiple_of(s * 2 * T + T - EDGE, EDGE), EDGE + T)
 
     def pcol(g):
         return slice(g * PAIR, (g + 1) * PAIR)
@@ -260,6 +264,12 @@
     for g in range(1, groups):
         spread_out(proj_of(g), pj_send.at[g])
 
+    pieces = dpb.shape[0]
+    dpb[:, 0:EDGE, :] = jnp.zeros((pieces, EDGE, LANES), f32)
+    dpb[:, EDGE + T : EDGE + T + NEXT, :] = jnp.zeros((pieces, NEXT, LANES), f32)
+    for s in range(dp):
+        dpall[s * 2 * T : s * 2 * T + T - EDGE, :] = jnp.zeros((T - EDGE, dpall.shape[1]), bf16)
+
     @pl.when(first)
     def _():
         val[0:EDGE, :] = jnp.zeros((EDGE, W), bf16)
@@ -272,7 +282,7 @@
         cin[1] = jnp.zeros((STATE, W), bf16)
         gin[1] = jnp.zeros(gin.shape[1:], bf16)
         dvb[:, T : T + NEXT, :] = jnp.zeros((dvb.shape[0], NEXT, LANES), f32)
-        dpb[:, T : T + NEXT, :] = jnp.zeros((dpb.shape[0], NEXT, LANES), f32)
+        dpn[...] = jnp.zeros(dpn.shape, f32)
 
     for load in small:
         load.wait()
@@ -315,10 +325,10 @@
             total = total + taps[i : i + 1, at] * buf[k, EDGE - 3 + i : EDGE - 3 + i + T, :]
         return total
 
-    def conv_back(buf, k, taps, at):
-        total = taps[3:4, at] * buf[k, 0:T, :]
+    def conv_back(buf, k, taps, at, start=0, count=T):
+        total = taps[3:4, at] * buf[k, start : start + count, :]
         for i in range(3):
-            total = total + taps[i : i + 1, at] * buf[k, 3 - i : 3 - i + T, :]
+            total = total + taps[i : i + 1, at] * buf[k, start + 3 - i : start + 3 - i + count, :]
         return total
 
     def before_pair(g):
@@ -417,12 +427,15 @@
     at_end = (z == 0) | (z == sp - 1)
 
     def go_next(kind, g):
-        buf = (dpb, dvb)[kind]
-        n = (2, tiles)[kind]
-        part = buf.at[g * n : (g + 1) * n]
+        if kind == 0:
+            part = slice(2 * g, 2 * g + 2)
+            src, dst = dpb.at[part, EDGE : EDGE + NEXT, :], dpn.at[part]
+        else:
+            part = slice(g * tiles, (g + 1) * tiles)
+            src, dst = dvb.at[part, 0:NEXT, :], dvb.at[part, T : T + NEXT, :]
         return remote(
-            part.at[:, 0:NEXT, :],
-            part.at[:, T : T + NEXT, :],
+            src,
+            dst,
             nx_sem.at[0, kind, g],
             nx_sem.at[1, kind, g],
             {"sp": below},
@@ -445,26 +458,26 @@
         dg = dgs[g]
         d_b = mm(dg, cc, TN) + mm(xeb[:, lanes], cin[1, :, lanes], NT)
         d_c = mm(dg, b, NN) + mm(edy[:, lanes], cin[0, :, lanes], NT)
-        dpb[2 * g, 0:T, :] = d_b * slp[2 * g]
-        dpb[2 * g + 1, 0:T, :] = d_c * slp[2 * g + 1]
+        for k, part in ((2 * g, d_b), (2 * g + 1, d_c)):
+            at = slice(k * LANES, (k + 1) * LANES)
+            dpb[k, EDGE : EDGE + T, :] = part * slp[k]
+            dpall[sent_rows(d), at] = conv_back(dpb, k, tap_p, at, 0, EDGE + T).astype(bf16)
+            spread_out(go_dpair(k), dg_send.at[k])
         send_next(0, g)
 
-    def go_dpair(g):
+    def go_dpair(k):
         def go(s, to, ss):
-            at = dpall.at[trow(s), pcol(g)]
-            return remote(at, at, ss, dg_recv.at[g, s], {"dp": to})
+            at = dpall.at[sent_rows(s), k * LANES : (k + 1) * LANES]
+            return remote(at, at, ss, dg_recv.at[k, s], {"dp": to})
 
         return go
 
     def pair_back(g):
         take_next(0, g)
-        for i in range(2):
-            k = 2 * g + i
+        for k in range(2 * g, 2 * g + 2):
             at = slice(k * LANES, (k + 1) * LANES)
-            grad = conv_back(dpb, k, tap_p, at).astype(bf16)
-            dpair[:, at] = grad
-            dpall[trow(d), at] = grad
-        spread_out(go_dpair(g), dg_send.at[g])
+            dpb[k, EDGE + T : EDGE + T + NEXT, :] = dpn[k]
+            dpair[:, at] = conv_back(dpb, k, tap_p, at, EDGE).astype(bf16)
 
     def value_grads(g):
         b = bc[2 * g]
@@ -512,23 +525,25 @@
 
     def go_nt(to):
         return remote(
-            nt.at[prow(to), :], ntall.at[:, trow(d)], nt_send.at[to], nt_recv.at[d], {"dp": to}
+            nt.at[prow(to), :], ntall.at[:, twice(d)], nt_send.at[to], nt_recv.at[d], {"dp": to}
         )
 
     def nt_from(s):
-        return remote(nt.at[prow(d), :], ntall.at[:, trow(s)], nt_send.at[s], nt_recv.at[s], {"dp": s})
+        return remote(nt.at[prow(d), :], ntall.at[:, twice(s)], nt_send.at[s], nt_recv.at[s], {"dp": s})
 
     def send_normed():
         for k in range(width // LANES):
             at = slice(k * LANES, (k + 1) * LANES)
-            nt[at, :] = nrm[EDGE : EDGE + T, at].T
+            nt[at, T : 2 * T] = nrm[EDGE : EDGE + T, at].T
+            edge = jnp.concatenate([jnp.zeros((T - EDGE, LANES), bf16), nrm[0:EDGE, at]], axis=0)
+            nt[at, 0:T] = edge.T
         for off in range(1, dp):
             go_nt(lax.rem(d + off, dp)).start()
-        ntall[:, trow(d)] = nt[prow(d), :]
+        ntall[:, twice(d)] = nt[prow(d), :]
 
     def row_part(k):
-        g, i = divmod(k, cuts)
-        return slice(i * (R // cuts), (i + 1) * (R // cuts)), pcol(g)
+        p, i = divmod(k, cuts)
+        return slice(i * (R // cuts), (i + 1) * (R // cuts)), slice(p * LANES, (p + 1) * LANES)
 
     def go_rows(q, k):
         r, c = row_part(k)
@@ -548,10 +563,10 @@
             gout[q, r, c] = (gin[q, r, c].astype(f32) + gpl[r, c]).astype(bf16)
             go_rows(q, k).start()
 
-    def rows_ends(g):
+    def rows_ends(p):
         @pl.when(at_end)
         def _():
-            for k in range(g * cuts, (g + 1) * cuts):
+            for k in range(p * cuts, (p + 1) * cuts):
                 rows_step(early, k)
 
     def rows_early(k):
@@ -559,9 +574,12 @@
         def _():
             rows_step(early, k)
 
-    def rows_product(g):
-        take_rest(go_dpair(g), dg_relay.at[g])
-        gpl[:, pcol(g)] = mm(ntall[...], dpall[:, pcol(g)], NN)
+    def rows_product(p):
+        pass_on(go_dpair(p), dg_send.at[p], dg_relay.at[p])
+        take_rest(go_dpair(p), dg_relay.at[p])
+        at = slice(p * LANES, (p + 1) * LANES)
+        gpl[:, at] = mm(ntall[...], dpall[:, at], NN)
+        rows_ends(p)
 
     def rows_total(k):
         r, c = row_part(k)
@@ -612,37 +630,41 @@
         if (i + 1) % chunks == 0:
             g = i // chunks
             pair_grads(g)
-            pair_back(g)
             if g + 1 < groups:
                 local_mix(g + 1)
 
     for s in range(1, dp):
         nt_from(lax.rem(d + s, dp)).wait_recv()
-    sent = 0
     for g in range(groups):
-        pass_on(go_dpair(g), dg_send.at[g], dg_relay.at[g])
-        while sent < g * cuts:
-            rows_early(sent)
-            sent += 1
-        rows_product(g)
-        rows_ends(g)
-        value_grads(g)
+        rows_product(2 * g)
+        rows_product(2 * g + 1)
+        if g + 1 < groups:
+            value_grads(g)
+    tail = groups - 1
+    for k in range(2 * tail * cuts):
+        rows_early(k)
+    value_grads(tail)
+    for g in range(groups):
+        pair_back(g)
     for k in range(width // 512):
         at = slice(k * 512, (k + 1) * 512)
         gn[:, at] = mm(dpair[...], proj[at, :], NT).astype(bf16)
-    while sent < groups * cuts:
-        rows_early(sent)
-        sent += 1
+    for k in range(2 * tail * cuts, pieces * cuts):
+        rows_early(k)
+    for k in range(2 * tail * cuts):
+        rows_step(late, k)
+        rows_total(k)
     for g in range(groups):
         value_back(g)
     step_grads()
-    for k in range(groups * cuts):
+    for k in range(2 * tail * cuts, pieces * cuts):
         rows_step(late, k)
         rows_total(k)
 
     for g in range(groups):
         drain(proj_of(g), pj_send.at[g], pj_relay.at[g])
-        drain(go_dpair(g), dg_send.at[g], dg_relay.at[g])
+    for k in range(pieces):
+        drain(go_dpair(k), dg_send.at[k], dg_relay.at[k])
     for off in range(1, dp):
         go_nt(lax.rem(d + off, dp)).wait_send()
 
@@ -662,7 +684,7 @@
         def _():
             for i in range(groups * chunks):
                 go_state(q, i).wait_send()
-            for k in range(groups * cuts):
+            for k in range(pieces * cuts):
                 go_rows(q, k).wait_send()
 
 
@@ -717,8 +739,8 @@
         V((T, W), bf16),
         V((T, W), bf16),
         V((width, cols), bf16),
-        V((width, T), bf16),
-        V((R, dp * T), bf16),
+        V((width, 2 * T), bf16),
+        V((R, dp * 2 * T), bf16),
         V((T, W), bf16),
         V((vt, EDGE + T, LANES), f32),
         V((T, W), f32),
@@ -741,9 +763,10 @@
         V((T, W), f32),
         V((2, T + NEXT, W), f32),
         V((vt, T + NEXT, LANES), f32),
-        V((pt, T + NEXT, LANES), f32),
+        V((pt, EDGE + T + NEXT, LANES), f32),
+        V((pt, NEXT, LANES), f32),
         V((T, cols), bf16),
-        V((dp * T, cols), bf16),
+        V((dp * 2 * T, cols), bf16),
         V((R, cols), f32),
         V((2, R, cols), bf16),
         V((2, R, cols), bf16),
@@ -757,11 +780,11 @@
         dma((2, 2, groups)),
         dma((dp,)),
         dma((dp,)),
-        dma((groups, dp)),
-        dma((groups, dp)),
-        dma((groups, dp)),
-        dma((2, groups * cuts)),
-        dma((2, groups * cuts)),
+        dma((pt, dp)),
+        dma((pt, dp)),
+        dma((pt, dp)),
+        dma((2, pt * cuts)),
+        dma((2, pt * cuts)),
     ]
     gn, gv, gg, gs, gp = pl.pallas_call(
         functools.partial(mixer_kernel, sp, dp, heads, groups, chunks, cuts),

time: 64.5 us -> 58.4 us (0.905)
  Pallas kernels: 63.7 us -> 57.6 us
    pallas_call x1, Pallas kernels: 62.4 us -> 56.2 us  [per_device(): pl.pallas_call(functools.partial(mixer_kernel, sp, dp, heads, groups, chu...]
where the time goes in v3:
time: 58.4 us; the launch traced here: 58.2 us
  Pallas kernels  57.6 us (99%)
  between operations  0.64 us (1%)
    pallas_call x1, Pallas kernels, per_device(): pl.pallas_call(functools.partial(mixer_kernel, sp, dp, heads, groups, chu...  56.2 us
    pallas_call x1, Pallas kernels, per_device(): pl.pallas_call(place_kernel, out_shape=tuple((jax.ShapeDtypeStruct(r.shap...  1.36 us

profile of v3, /device:TPU:0, one launch (start us, length us, event | category | flops | bytes accessed | tf_op | source)
XLA Modules:
  0.0 58.2 jit_solution(13623112186744968411)
XLA Ops:
  0.6 56.2 %shard_map.146 = (bf16[128,2048]{1,0:T(8,128)(2,1)S(1)}, bf16[128,2048]{1,0:T(8,128)(2,1)S(1)}, bf16[128,2048]{1,0:T(8,128)(2,1)S(1)}, bf16[32,128]{1,0:T(8,128)(2,1)S(1)}, f32[256,512]{1,0:T(8,128)S(1)}) custom-call(bf16[128,2048]{1,0:T(8,128)(2,1)} %bitcast.16, bf16[128,2048]{1,0:T(8,128)(2,1)} %bitcast.17, bf16[128,2048]{1,0:T(8,128)(2,1)} %bitcast.18, ...), custom_call_target="tpu_custom_call" | custom-call | tf_op jit(solution)/shard_map/pallas_call | solution.py:789
  56.9 1.4 %shard_map.147 = (bf16[128,2048]{1,0:T(8,128)(2,1)}, bf16[128,2048]{1,0:T(8,128)(2,1)}, bf16[128,2048]{1,0:T(8,128)(2,1)}, bf16[32,128]{1,0:T(8,128)(2,1)}, f32[256,512]{1,0:T(8,128)}) custom-call(bf16[128,2048]{1,0:T(8,128)(2,1)S(1)} %get-tuple-element.15.refs_0_, bf16[128,2048]{1,0:T(8,128)(2,1)S(1)} %get-tuple-element.16.refs_1_, ...), custom_call_target="tpu_custom_call" | custom-call | tf_op jit(solution)/shard_map/pallas_call | solution.py:823

commit v4 on v3

--- a/solution.py
+++ b/solution.py
@@ -83,13 +83,13 @@
     slv,
     upslope,
     xb,
-    xeb,
-    edy,
+    tx,
     dec,
     dgs,
     gm,
     pairx,
     bc,
+    bct,
     slp,
     ee,
     car,
@@ -216,16 +216,24 @@
         return remote(at, at, ss, pj_recv.at[g, s], {"dp": to})
 
     def chip_peer(off):
-        return lax.rem(chip + off, nch) * 2 + core
+        if nch & (nch - 1):
+            return lax.rem(chip + off, nch) * 2 + core
+        to = chip
+        for bit in range(off.bit_length()):
+            if off >> bit & 1:
+                to = to + (1 - 2 * lax.rem(chip // 2**bit, 2)) * 2**bit
+        return to * 2 + core
+
+    far_first = sorted(range(1, nch), key=lambda off: (-bin(off).count("1"), off))
 
     def spread_out(go, send):
-        for off in range(1, nch):
+        for off in far_first:
             to = chip_peer(off)
             go(d, to, send.at[to]).start()
         go(d, sib, send.at[sib]).start()
 
     def pass_on(go, send, relay):
-        for off in range(1, nch):
+        for off in far_first:
             s = chip_peer(off)
             go(s, sib, relay.at[s]).wait_recv()
             go(s, sib, relay.at[s]).start()
@@ -347,8 +355,8 @@
             slv[:, at] = slope
             x = (u * spread(dt, j)).astype(bf16)
             xb[:, at] = x
-            xeb[:, at] = (x.astype(f32) * spread(te, j)).astype(bf16)
-            edy[:, at] = (spread(ea, j) * dy.astype(f32)).astype(bf16)
+            tx[0, :, at] = (x.astype(f32) * spread(te, j)).astype(bf16)
+            tx[1, :, at] = (spread(ea, j) * dy.astype(f32)).astype(bf16)
             ee[:, at] = spread(e_end, j)
             d_mix = mm(halves(dy), x, NT)
             for q in range(2):
@@ -357,7 +365,45 @@
                 decay = jnp.exp(jnp.where(causal, diff, -1e30))
                 dec[h] = decay
                 d_g = d_g + d_mix[q * T : (q + 1) * T] * decay
-        dgs[g] = d_g.astype(bf16)
+        dgs[g, 0] = d_g.astype(bf16)
+        dgs[g, 1] = d_g.T.astype(bf16)
+
+    def has_in(q):
+        return jnp.where(q == 0, z > 0, z < sp - 1)
+
+    def has_out(q):
+        return jnp.where(q == 0, z < sp - 1, z > 0)
+
+    def onward(q):
+        return lax.max(lax.min(z + 1 - 2 * q, sp - 1), 0)
+
+    def go_state(q, i):
+        lanes = slice(i * CW, (i + 1) * CW)
+        return remote(
+            cout.at[q, :, lanes], cin.at[q, :, lanes], ch_send.at[q, i], ch_recv.at[q, i], {"sp": onward(q)}
+        )
+
+    def chain_step(q, i):
+        lanes = slice(i * CW, (i + 1) * CW)
+
+        @pl.when(has_in(q))
+        def _():
+            go_state(q, i).wait_recv()
+
+        @pl.when(has_out(q))
+        def _():
+            total = cin[q, :, lanes].astype(f32) * ee[0:1, lanes] + car[q, :, lanes]
+            cout[q, :, lanes] = total.astype(bf16)
+            go_state(q, i).start()
+
+    def chain_early(i):
+        @pl.when(jnp.logical_not(at_end))
+        def _():
+            chain_step(early, i)
+
+    early = jnp.where(z < sp // 2, 0, 1)
+    late = 1 - early
+    at_end = (z == 0) | (z == sp - 1)
 
     def pair_stage(g):
         lanes = slice(g * GW, (g + 1) * GW)
@@ -368,12 +414,25 @@
             pairx[k] = pb[:, i * LANES : (i + 1) * LANES]
             act, slope = silu_parts(conv(pairx, k, tap_p, at))
             bc[k] = act.astype(bf16)
+            bct[k] = act.T.astype(bf16)
             slp[k] = slope
-        b = bc[2 * g]
-        cc = bc[2 * g + 1]
-        gm[g] = mm(cc, b, NT)
-        car[0, :, lanes] = mm(b, xeb[:, lanes], TN)
-        car[1, :, lanes] = mm(cc, edy[:, lanes], TN)
+
+        @pl.when(at_end)
+        def _():
+            for i in range(g * chunks, (g + 1) * chunks):
+                at = slice(i * CW, (i + 1) * CW)
+                cout[early, :, at] = mm(bct[2 * g + early], tx[early, :, at], NN).astype(bf16)
+
+                @pl.when(has_out(early))
+                def _():
+                    go_state(early, i).start()
+
+        @pl.when(jnp.logical_not(at_end))
+        def _():
+            for q in range(2):
+                car[q, :, lanes] = mm(bct[2 * g + q], tx[q, :, lanes], NN)
+
+        gm[g] = mm(bc[2 * g + 1], bct[2 * g], NN)
 
     def local_mix(g):
         gmat = gm[g]
@@ -382,49 +441,6 @@
             mixes = [(gmat * dec[2 * j + q]).astype(bf16) for q in range(2)]
             ybuf[:, at] = mm(jnp.concatenate(mixes, axis=1), halves(xb[:, at]), NN)
             dxl[:, at] = mm(jnp.concatenate(mixes, axis=0), halves(cot[:, at]), TN)
-
-    def has_in(q):
-        return jnp.where(q == 0, z > 0, z < sp - 1)
-
-    def has_out(q):
-        return jnp.where(q == 0, z < sp - 1, z > 0)
-
-    def onward(q):
-        return lax.max(lax.min(z + 1 - 2 * q, sp - 1), 0)
-
-    def go_state(q, i):
-        lanes = slice(i * CW, (i + 1) * CW)
-        return remote(
-            cout.at[q, :, lanes], cin.at[q, :, lanes], ch_send.at[q, i], ch_recv.at[q, i], {"sp": onward(q)}
-        )
-
-    def chain_step(q, i):
-        lanes = slice(i * CW, (i + 1) * CW)
-
-        @pl.when(has_in(q))
-        def _():
-            go_state(q, i).wait_recv()
-
-        @pl.when(has_out(q))
-        def _():
-            total = cin[q, :, lanes].astype(f32) * ee[0:1, lanes] + car[q, :, lanes]
-            cout[q, :, lanes] = total.astype(bf16)
-            go_state(q, i).start()
-
-    def chain_ends(g):
-        @pl.when(at_end)
-        def _():
-            for i in range(g * chunks, (g + 1) * chunks):
-                chain_step(early, i)
-
-    def chain_early(i):
-        @pl.when(jnp.logical_not(at_end))
-        def _():
-            chain_step(early, i)
-
-    early = jnp.where(z < sp // 2, 0, 1)
-    late = 1 - early
-    at_end = (z == 0) | (z == sp - 1)
 
     def go_next(kind, g):
         if kind == 0:
@@ -451,23 +467,24 @@
         def _():
             go_next(kind, g).wait_recv()
 
-    def pair_grads(g):
+    def piece(g, q):
+        return 2 * g + 1 - q
+
+    def lanes_of(k):
+        return pl.ds(pl.multiple_of(k * LANES, LANES), LANES)
+
+    def pair_grads(g, q):
         lanes = slice(g * GW, (g + 1) * GW)
-        b = bc[2 * g]
-        cc = bc[2 * g + 1]
-        dg = dgs[g]
-        d_b = mm(dg, cc, TN) + mm(xeb[:, lanes], cin[1, :, lanes], NT)
-        d_c = mm(dg, b, NN) + mm(edy[:, lanes], cin[0, :, lanes], NT)
-        for k, part in ((2 * g, d_b), (2 * g + 1, d_c)):
-            at = slice(k * LANES, (k + 1) * LANES)
-            dpb[k, EDGE : EDGE + T, :] = part * slp[k]
-            dpall[sent_rows(d), at] = conv_back(dpb, k, tap_p, at, 0, EDGE + T).astype(bf16)
-            spread_out(go_dpair(k), dg_send.at[k])
-        send_next(0, g)
+        k = piece(g, q)
+        part = mm(dgs[g, q], bc[2 * g + q], NN) + mm(tx[1 - q, :, lanes], cin[q, :, lanes], NT)
+        dpb[k, EDGE : EDGE + T, :] = part * slp[k]
+        at = lanes_of(k)
+        dpall[sent_rows(d), at] = conv_back(dpb, k, tap_p, at, 0, EDGE + T).astype(bf16)
+        spread_out(go_dpair(k), dg_send.at[k])
 
     def go_dpair(k):
         def go(s, to, ss):
-            at = dpall.at[sent_rows(s), k * LANES : (k + 1) * LANES]
+            at = dpall.at[sent_rows(s), lanes_of(k)]
             return remote(at, at, ss, dg_recv.at[k, s], {"dp": to})
 
         return go
@@ -541,49 +558,53 @@
             go_nt(lax.rem(d + off, dp)).start()
         ntall[:, twice(d)] = nt[prow(d), :]
 
-    def row_part(k):
-        p, i = divmod(k, cuts)
-        return slice(i * (R // cuts), (i + 1) * (R // cuts)), slice(p * LANES, (p + 1) * LANES)
-
-    def go_rows(q, k):
-        r, c = row_part(k)
+    def row_part(p, i):
+        return slice(i * (R // cuts), (i + 1) * (R // cuts)), lanes_of(p)
+
+    def go_rows(q, p, i):
+        r, c = row_part(p, i)
+        k = p * cuts + i
         return remote(
             gout.at[q, r, c], gin.at[q, r, c], gc_send.at[q, k], gc_recv.at[q, k], {"sp": onward(q)}
         )
 
-    def rows_step(q, k):
-        r, c = row_part(k)
-
-        @pl.when(has_in(q))
-        def _():
-            go_rows(q, k).wait_recv()
-
-        @pl.when(has_out(q))
-        def _():
-            gout[q, r, c] = (gin[q, r, c].astype(f32) + gpl[r, c]).astype(bf16)
-            go_rows(q, k).start()
+    def rows_step(q, p):
+        for i in range(cuts):
+            r, c = row_part(p, i)
+
+            @pl.when(has_in(q))
+            def _():
+                go_rows(q, p, i).wait_recv()
+
+            @pl.when(has_out(q))
+            def _():
+                gout[q, r, c] = (gin[q, r, c].astype(f32) + gpl[r, c]).astype(bf16)
+                go_rows(q, p, i).start()
 
     def rows_ends(p):
         @pl.when(at_end)
         def _():
-            for k in range(p * cuts, (p + 1) * cuts):
-                rows_step(early, k)
-
-    def rows_early(k):
+            rows_step(early, p)
+
+    def rows_early(p):
         @pl.when(jnp.logical_not(at_end))
         def _():
-            rows_step(early, k)
-
-    def rows_product(p):
+            rows_step(early, p)
+
+    def take_normed():
+        for s in range(1, dp):
+            nt_from(lax.rem(d + s, dp)).wait_recv()
+
+    def rows_of(p):
         pass_on(go_dpair(p), dg_send.at[p], dg_relay.at[p])
         take_rest(go_dpair(p), dg_relay.at[p])
-        at = slice(p * LANES, (p + 1) * LANES)
+        at = lanes_of(p)
         gpl[:, at] = mm(ntall[...], dpall[:, at], NN)
         rows_ends(p)
 
-    def rows_total(k):
-        r, c = row_part(k)
-        gp[r, c] = gin[0, r, c].astype(f32) + gpl[r, c] + gin[1, r, c].astype(f32)
+    def rows_total(g):
+        at = pcol(g)
+        gp[:, at] = gin[0, :, at].astype(f32) + gpl[:, at] + gin[1, :, at].astype(f32)
 
     def pass_proj(g):
         pass_on(proj_of(g), pj_send.at[g], pj_relay.at[g])
@@ -607,7 +628,6 @@
 
     pass_proj(0)
     pair_stage(0)
-    chain_ends(0)
     local_mix(0)
     send_normed()
     done_early = 0
@@ -618,48 +638,56 @@
             done_early += 1
         take_rest(proj_of(g), pj_relay.at[g])
         pair_stage(g)
-        chain_ends(g)
 
     order = [(i, 0, i) for i in range(done_early, groups * chunks)]
     order += [(i + chunks // 2 + 0.5, 1, i) for i in range(groups * chunks)]
     for _, kind, i in sorted(order):
+        g = i // chunks
+        ends_group = (i + 1) % chunks == 0
         if kind == 0:
             chain_early(i)
-            continue
-        chain_step(late, i)
-        if (i + 1) % chunks == 0:
-            g = i // chunks
-            pair_grads(g)
-            if g + 1 < groups:
-                local_mix(g + 1)
-
-    for s in range(1, dp):
-        nt_from(lax.rem(d + s, dp)).wait_recv()
-    for g in range(groups):
-        rows_product(2 * g)
-        rows_product(2 * g + 1)
-        if g + 1 < groups:
-            value_grads(g)
+            if ends_group:
+                pair_grads(g, early)
+        else:
+            chain_step(late, i)
+            if g > 0 and i % chunks == chunks // 2:
+                if g == 1:
+                    take_normed()
+                rows_of(piece(g - 1, early))
+            if ends_group:
+                pair_grads(g, late)
+                send_next(0, g)
+                if g + 1 < groups:
+                    local_mix(g + 1)
+
     tail = groups - 1
-    for k in range(2 * tail * cuts):
-        rows_early(k)
+    for g in range(tail):
+        rows_of(piece(g, late))
+    rows_of(piece(tail, early))
+    for g in range(tail):
+        rows_early(piece(g, early))
+        value_grads(g)
+    rows_of(piece(tail, late))
     value_grads(tail)
+    for g in range(tail):
+        rows_step(late, piece(g, late))
+        rows_early(piece(g, late))
+    rows_early(piece(tail, early))
     for g in range(groups):
         pair_back(g)
     for k in range(width // 512):
         at = slice(k * 512, (k + 1) * 512)
         gn[:, at] = mm(dpair[...], proj[at, :], NT).astype(bf16)
-    for k in range(2 * tail * cuts, pieces * cuts):
-        rows_early(k)
-    for k in range(2 * tail * cuts):
-        rows_step(late, k)
-        rows_total(k)
+    for g in range(tail):
+        rows_step(late, piece(g, early))
+        rows_total(g)
+    rows_early(piece(tail, late))
+    rows_step(late, piece(tail, late))
     for g in range(groups):
         value_back(g)
     step_grads()
-    for k in range(2 * tail * cuts, pieces * cuts):
-        rows_step(late, k)
-        rows_total(k)
+    rows_step(late, piece(tail, early))
+    rows_total(tail)
 
     for g in range(groups):
         drain(proj_of(g), pj_send.at[g], pj_relay.at[g])
@@ -684,8 +712,9 @@
         def _():
             for i in range(groups * chunks):
                 go_state(q, i).wait_send()
-            for k in range(pieces * cuts):
-                go_rows(q, k).wait_send()
+            for k in range(pieces):
+                for i in range(cuts):
+                    go_rows(q, k, i).wait_send()
 
 
 def place_kernel(*refs):
@@ -747,13 +776,13 @@
         V((T, W), f32),
         V((T, W), f32),
         V((T, W), bf16),
-        V((T, W), bf16),
-        V((T, W), bf16),
+        V((2, T, W), bf16),
         V((heads, T, T), f32),
-        V((groups, T, T), bf16),
+        V((groups, 2, T, T), bf16),
         V((groups, T, T), f32),
         V((pt, EDGE + T, LANES), f32),
         V((pt, T, LANES), bf16),
+        V((pt, LANES, T), bf16),
         V((pt, T, LANES), f32),
         V((1, W), f32),
         V((2, STATE, W), f32),

time: 58.4 us -> 56.3 us (0.964)
  Pallas kernels: 57.6 us -> 55.5 us
    pallas_call x1, Pallas kernels: 56.2 us -> 54.1 us  [per_device(): pl.pallas_call(functools.partial(mixer_kernel, sp, dp, heads, groups, chu...]
where the time goes in v4:
time: 56.3 us; the launch traced here: 56.1 us
  Pallas kernels  55.5 us (99%)
  between operations  0.64 us (1%)
    pallas_call x1, Pallas kernels, per_device(): pl.pallas_call(functools.partial(mixer_kernel, sp, dp, heads, groups, chu...  54.1 us
    pallas_call x1, Pallas kernels, per_device(): pl.pallas_call(place_kernel, out_shape=tuple((jax.ShapeDtypeStruct(r.shap...  1.36 us

profile of v4, /device:TPU:0, one launch (start us, length us, event | category | flops | bytes accessed | tf_op | source)
XLA Modules:
  0.0 56.1 jit_solution(11580774548110087026)
XLA Ops:
  0.6 54.1 %shard_map.146 = (bf16[128,2048]{1,0:T(8,128)(2,1)S(1)}, bf16[128,2048]{1,0:T(8,128)(2,1)S(1)}, bf16[128,2048]{1,0:T(8,128)(2,1)S(1)}, bf16[32,128]{1,0:T(8,128)(2,1)S(1)}, f32[256,512]{1,0:T(8,128)S(1)}) custom-call(bf16[128,2048]{1,0:T(8,128)(2,1)} %bitcast.16, bf16[128,2048]{1,0:T(8,128)(2,1)} %bitcast.17, bf16[128,2048]{1,0:T(8,128)(2,1)} %bitcast.18, ...), custom_call_target="tpu_custom_call" | custom-call | tf_op jit(solution)/shard_map/pallas_call | solution.py:818
  54.8 1.4 %shard_map.147 = (bf16[128,2048]{1,0:T(8,128)(2,1)}, bf16[128,2048]{1,0:T(8,128)(2,1)}, bf16[128,2048]{1,0:T(8,128)(2,1)}, bf16[32,128]{1,0:T(8,128)(2,1)}, f32[256,512]{1,0:T(8,128)}) custom-call(bf16[128,2048]{1,0:T(8,128)(2,1)S(1)} %get-tuple-element.15.refs_0_, bf16[128,2048]{1,0:T(8,128)(2,1)S(1)} %get-tuple-element.16.refs_1_, ...), custom_call_target="tpu_custom_call" | custom-call | tf_op jit(solution)/shard_map/pallas_call | solution.py:852

commit v5 on v4

--- a/solution.py
+++ b/solution.py
@@ -717,9 +717,17 @@
                     go_rows(q, k, i).wait_send()
 
 
-def place_kernel(*refs):
+def place_kernel(parts, *refs):
     sources, targets, sem = refs[0:5], refs[5:10], refs[10]
-    copies = [pltpu.make_async_copy(sources[k], targets[k], sem.at[k]) for k in range(5)]
+    copies = []
+    for k in range(5):
+        rows = sources[k].shape[0]
+        count = parts if rows % (16 * parts) == 0 else 1
+        for i in range(count):
+            at = slice(i * (rows // count), (i + 1) * (rows // count))
+            copies.append(
+                pltpu.make_async_copy(sources[k].at[at, :], targets[k].at[at, :], sem.at[k, i])
+            )
     for copy in copies:
         copy.start()
     for copy in copies:
@@ -850,11 +858,11 @@
     )
     results = (gn, gv, gg, gs, gp)
     gn, gv, gg, gs, gp = pl.pallas_call(
-        place_kernel,
+        functools.partial(place_kernel, 4),
         out_shape=tuple(jax.ShapeDtypeStruct(r.shape, r.dtype) for r in results),
         in_specs=[vmem] * 5,
         out_specs=(hbm,) * 5,
-        scratch_shapes=[dma((5,))],
+        scratch_shapes=[dma((5, 4))],
         compiler_params=pltpu.CompilerParams(vmem_limit_bytes=8 * 1024 * 1024),
     )(*results)
     return (gn[None], gv[None], gg[None], gs.T[None], gp)

time: 56.3 us -> 56.4 us (level)
  no operation moved by 1% of the time
where the time goes in v5:
time: 56.4 us; the launch traced here: 56.3 us
  Pallas kernels  55.6 us (99%)
  between operations  0.64 us (1%)
    pallas_call x1, Pallas kernels, per_device(): pl.pallas_call(functools.partial(mixer_kernel, sp, dp, heads, groups, chu...  54.1 us
    pallas_call x1, Pallas kernels, per_device(): pl.pallas_call(functools.partial(place_kernel, 4), out_shape=tuple((jax.S...  1.48 us

profile of v5, /device:TPU:0, one launch (start us, length us, event | category | flops | bytes accessed | tf_op | source)
XLA Modules:
  0.0 56.3 jit_solution(16222789889970169469)
XLA Ops:
  0.6 54.1 %shard_map.146 = (bf16[128,2048]{1,0:T(8,128)(2,1)S(1)}, bf16[128,2048]{1,0:T(8,128)(2,1)S(1)}, bf16[128,2048]{1,0:T(8,128)(2,1)S(1)}, bf16[32,128]{1,0:T(8,128)(2,1)S(1)}, f32[256,512]{1,0:T(8,128)S(1)}) custom-call(bf16[128,2048]{1,0:T(8,128)(2,1)} %bitcast.16, bf16[128,2048]{1,0:T(8,128)(2,1)} %bitcast.17, bf16[128,2048]{1,0:T(8,128)(2,1)} %bitcast.18, ...), custom_call_target="tpu_custom_call" | custom-call | tf_op jit(solution)/shard_map/pallas_call | solution.py:826
  54.8 1.5 %shard_map.147 = (bf16[128,2048]{1,0:T(8,128)(2,1)}, bf16[128,2048]{1,0:T(8,128)(2,1)}, bf16[128,2048]{1,0:T(8,128)(2,1)}, bf16[32,128]{1,0:T(8,128)(2,1)}, f32[256,512]{1,0:T(8,128)}) custom-call(bf16[128,2048]{1,0:T(8,128)(2,1)S(1)} %get-tuple-element.15.refs_0_, bf16[128,2048]{1,0:T(8,128)(2,1)S(1)} %get-tuple-element.16.refs_1_, ...), custom_call_target="tpu_custom_call" | custom-call | tf_op jit(solution)/shard_map/pallas_call | solution.py:860
